TPU v7x, 32 devices: a whole 2x2x4 slice. The times are simulated.
32 devices in a mesh: sp: 4 (over z), fs: 4 (over y, x), tp: 2 (over core).
Axes of the slice: x: 2, y: 2, z: 4, core: 2. Of those that a mesh axis runs over, the one named last changes fastest.
Arguments:
- statespace_input: bfloat16 [4, 1536, 2048], P('fs', 'sp', 'tp'), may hold values from -6 to 6
- output_gate_input: bfloat16 [4, 1536, 2048], P('fs', 'sp', 'tp'), may hold values from -6 to 6
- state_input_projection: bfloat16 [4, 1536, 512], P('fs', 'sp', 'tp'), may hold values from -6 to 6
- state_output_projection: bfloat16 [4, 1536, 512], P('fs', 'sp', 'tp'), may hold values from -6 to 6
- step_size_input: bfloat16 [4, 1536, 32], P('fs', 'sp', 'tp'), may hold values from -5 to 5
- added_log_decay: float32 [4, 1536, 32], P('fs', 'sp', 'tp'), may hold values from -0.7 to 0
- logarithm_rates: float32 [32], replicated, may hold values from -20 to -2.9
- head_channel_taps: bfloat16 [4, 2048], replicated, may hold values from -3 to 3
- input_projection_taps: bfloat16 [4, 512], replicated, may hold values from -3 to 3
- output_projection_taps: bfloat16 [4, 512], replicated, may hold values from -3 to 3
- input_projection_bias: bfloat16 [512], replicated, may hold values from -0.59765625 to -0.19921875
- group_norm_gain: bfloat16 [2048], replicated, may hold values from 0.099609375 to 1.8984375
- pooling_input: bfloat16 [4, 1536, 1024], P('fs', 'sp', 'tp'), may hold values from -6 to 6
- pooling_group_weight: bfloat16 [4, 256, 256], replicated, may hold values from -0.375 to 0.375
- pooling_channel_scale: bfloat16 [1024], replicated, may hold values from 0.099609375 to 1.8984375
- statespace_output_weight: bfloat16 [2048, 4096], P('tp', ('sp', 'fs')), may hold values from -8 to 8
- pooling_output_weight: bfloat16 [1024, 4096], P('tp', ('sp', 'fs')), may hold values from -8 to 8
- output_norm_gain: bfloat16 [4096], replicated, may hold values from 0.099609375 to 1.8984375
Outputs:
- output: bfloat16 [4, 1536, 4096], P('fs', 'sp', 'tp')
All inputs are finite; a program needn't handle non-finite values.
Results may differ from a plain program's by a relative error of at most 0.02.
Values may be sent and summed in bfloat16 or wider, within the bound.
A program may use at most 128 MiB of HBM per device.

v0:
```python
import functools

import jax
import jax.numpy as jnp
from jax import lax
from jax.experimental import pallas as pl
from jax.experimental.pallas import tpu as pltpu
from jax.sharding import PartitionSpec as P

D = 4096
HEAD_DIM = 64
STATE = 128
CONV = 4
BLOCK = 128
POOL_GROUPS = 4
POOL_GROUP = 256


eps = 1e-06


def passed_along(block, axis, distance):
    devices = range(lax.axis_size(axis))
    route = [(i - distance, i) for i in devices if i - distance in devices]
    return lax.ppermute(block, axis, route)


def entering_2(array, axis, join, neutral):
    place = lax.axis_index(axis)
    gathered = jax.tree.map(
        lambda a, kind: lax.all_gather(a.astype(kind), axis), array, (jnp.bfloat16, jnp.bfloat16)
    )
    state = jax.tree.map(lambda a, e: jnp.zeros_like(a) + jnp.asarray(e, a.dtype), array, neutral)

    def one(lap, state):
        return join(
            state,
            jax.tree.map(
                lambda a, own: lax.dynamic_index_in_dim(a, lap, 0, False).astype(own.dtype),
                gathered,
                array,
            ),
        )

    return lax.fori_loop(0, place, one, state)


MESH_IDS = pl.DeviceIdType.MESH
EXACT = lax.Precision.HIGHEST


def ring_place(index, size):
    if size != 4:
        return index
    return index + (index // 2) * (1 - 2 * (index % 2))


class Gather:
    def __init__(self, own, whole, sends, arrivals, sp_size, fs_size):
        self.own, self.whole = own, whole
        self.sends, self.arrivals = sends, arrivals
        self.width = own.shape[1]
        self.sp_size, self.fs_size = sp_size, fs_size
        self.sp_me = lax.axis_index("sp")
        self.fs_me = ring_place(lax.axis_index("fs"), fs_size)
        rows = own.shape[0]
        self.cut = rows * 3 // 4 // 64 * 64
        self.keys = {}
        self.fs_last = fs_size // 2
        self.fs_offsets = [0]
        for step in range(1, self.fs_last + 1):
            self.fs_offsets.append(-step)
            if not self.halved(step):
                self.fs_offsets.append(step)

    def halved(self, step):
        return self.fs_size % 2 == 0 and step == self.fs_last

    def fs_at(self, offset):
        return ring_place(lax.rem(self.fs_me + offset + 2 * self.fs_size, self.fs_size), self.fs_size)

    def copy(self, part, stage, cross, step, way):
        on_sp = part == stage
        low, high = (0, self.cut) if part == 0 else (self.cut, self.own.shape[0])
        if not on_sp and self.halved(step):
            mid = low + (high - low) // 2
            low, high = (low, mid) if way == 1 else (mid, high)
        rows = pl.ds(low, high - low)
        off = -way * (step - 1)
        sp_off, fs_off = (off, cross) if on_sp else (cross, off)
        at = ((self.sp_me + sp_off) * self.fs_size + self.fs_at(fs_off)) * self.width
        cols = pl.ds(pl.multiple_of(at, self.width), self.width)
        first = sp_off == 0 and fs_off == 0
        spot = self.keys.setdefault((part, stage, cross, step, way), len(self.keys))
        return pltpu.make_async_remote_copy(
            src_ref=self.own.at[rows] if first else self.whole.at[rows, cols],
            dst_ref=self.whole.at[rows, cols],
            send_sem=self.sends.at[spot],
            recv_sem=self.arrivals.at[spot],
            device_id={"sp": self.sp_me + way} if on_sp else {"fs": self.fs_at(way)},
            device_id_type=MESH_IDS,
        )

    def when(self, part, stage, cross, step, way, arriving):
        if part == stage:
            gone = step if arriving else step - 1
            origin = self.sp_me - way * gone
            far = self.sp_me if arriving else self.sp_me + way
            checks = [origin >= 0, origin < self.sp_size, far >= 0, far < self.sp_size]
        elif cross:
            checks = [self.sp_me + cross >= 0, self.sp_me + cross < self.sp_size]
        else:
            return None
        return functools.reduce(jnp.logical_and, checks)

    def each(self, part, stage, cross, step, arriving, act):
        last = self.sp_size - 1 if part == stage else self.fs_last
        if not 1 <= step <= last:
            return
        for way in (1, -1):
            key = (part, stage, cross, step, way)
            here = self.when(*key, arriving)

            def run(key=key):
                act(self.copy(*key))

            if here is None:
                run()
            else:
                pl.when(here)(run)

    def send(self, *key):
        self.each(*key, False, lambda copy: copy.start())

    def take(self, *key):
        self.each(*key, True, lambda copy: copy.wait_recv())

    def barrier(self):
        barrier = pltpu.get_barrier_semaphore()
        total = 0
        for far in range(1, self.sp_size):
            other = lax.rem(self.sp_me + far, self.sp_size)
            pl.semaphore_signal(barrier, inc=1, device_id={"sp": other}, device_id_type=MESH_IDS)
            total += 1
        if self.fs_size > 1:
            for way in (1, -1):
                other = self.fs_at(way)
                pl.semaphore_signal(
                    barrier, inc=1, device_id={"fs": other}, device_id_type=MESH_IDS
                )
                total += 1
        if total:
            pl.semaphore_wait(barrier, total)

    def pair(self, off):
        return [0] if off == 0 else [-off, off]

    def run(self):
        rounds = max(self.sp_size - 1, self.fs_last)
        self.send(0, 0, 0, 1)
        self.send(1, 0, 0, 1)
        self.send(0, 1, 0, 1)
        for step in range(1, rounds + 1):
            yield
            self.take(0, 0, 0, step)
            self.send(0, 0, 0, step + 1)
            if step < self.sp_size:
                for cross in self.pair(step):
                    self.send(0, 1, cross, 1)
            if step == 1:
                self.send(1, 1, 0, 1)
            self.take(1, 0, 0, step)
            self.send(1, 0, 0, step + 1)
            for cross in self.fs_offsets[1:]:
                if abs(cross) == step:
                    self.send(1, 1, cross, 1)
            yield
            if step <= self.sp_size:
                for cross in self.pair(step - 1):
                    self.take(0, 1, cross, 1)
                    self.send(0, 1, cross, 2)
            yield
            if step > self.fs_last:
                for cross in self.fs_offsets:
                    self.take(1, 1, cross, step - self.fs_last)
                    self.send(1, 1, cross, step - self.fs_last + 1)
        for late in range(rounds, self.sp_size):
            yield
            for cross in self.pair(late):
                self.take(0, 1, cross, 1)
                self.send(0, 1, cross, 2)
        for step in range(max(rounds - self.fs_last, 0) + 1, self.sp_size):
            for cross in self.fs_offsets:
                yield
                self.take(1, 1, cross, step)
                self.send(1, 1, cross, step + 1)
        for step in range(2, self.fs_last + 1):
            for off in range(self.sp_size):
                yield
                for cross in self.pair(off):
                    self.take(0, 1, cross, step)
                    self.send(0, 1, cross, step + 1)

    def finish(self):
        for key in list(self.keys):
            part, stage, cross, step, way = key
            here = self.when(*key, False)

            def run(key=key):
                self.copy(*key).wait_send()

            if here is None:
                run()
            else:
                pl.when(here)(run)


def hop_count(sp_size, fs_size):
    along, around = 2 * (sp_size - 1), 2 * (fs_size // 2)
    return along * (1 + fs_size) + around * (1 + 2 * sp_size - 1)


def silu(rows):
    return rows / (1.0 + jnp.exp(-rows))


def softplus(rows):
    return jnp.maximum(rows, 0.0) + jnp.log(1.0 + jnp.exp(-jnp.abs(rows)))


def mixers(sizes, refs, links):
    sp_size, tail = sizes
    (x_in, gate, bc_in, dt, dt_t, added, added_t, rates, rates_t, x_taps, bc_taps, bc_bias, gain,
     pool_in, pool_weight, pool_scale, reach, prior, channels, x_pad, bc_pad, pool_pad, x_conv,
     bc_conv, within, grown, local_in, state, ends, before, far_state, far_log) = refs
    sends, arrivals = links
    rows, inner = x_in.shape
    heads = dt.shape[1]
    wide = bc_in.shape[1] // 2
    groups = wide // STATE
    span = inner // groups
    blocks = rows // BLOCK
    sp_me = lax.axis_index("sp")
    x_pad[0:tail] = prior[:, 0:inner].astype(jnp.float32)
    bc_pad[0:tail] = prior[:, inner : inner + 2 * wide].astype(jnp.float32)
    pool_pad[0:tail] = prior[:, inner + 2 * wide :].astype(jnp.float32)
    x_pad[tail:] = x_in[...].astype(jnp.float32)
    bc_pad[tail:] = bc_in[...].astype(jnp.float32)
    pool_pad[tail:] = pool_in[...].astype(jnp.float32)
    step_all = softplus(dt[...].astype(jnp.float32))
    log_all = -step_all * jnp.exp(rates[...]) + added[...]
    step_flat = softplus(dt_t[...].astype(jnp.float32))
    log_flat = -step_flat * jnp.exp(rates_t[...]) + added_t[...]
    down = lax.broadcasted_iota(jnp.int32, (BLOCK, BLOCK), 0)
    across = lax.broadcasted_iota(jnp.int32, (BLOCK, BLOCK), 1)
    causal = down >= across
    lower = causal.astype(jnp.float32)
    upper = (down <= across).astype(jnp.float32)
    first_half = lax.broadcasted_iota(jnp.int32, (BLOCK, 2 * HEAD_DIM), 1) < HEAD_DIM
    yield

    def taps(pad, weights, at, cols):
        total = None
        for tap in range(CONV):
            begin = at * BLOCK + tail - CONV + 1 + tap
            term = pad[begin : begin + BLOCK, cols] * weights[tap : tap + 1, cols].astype(
                jnp.float32
            )
            total = term if total is None else total + term
        return total

    state[...] = jnp.zeros_like(state)
    for at in range(blocks):
        now = slice(at * BLOCK, (at + 1) * BLOCK)
        every = slice(0, 2 * wide)
        bc_conv[now] = silu(
            taps(bc_pad, bc_taps, at, every) + bc_bias[...].astype(jnp.float32)
        ).astype(jnp.bfloat16)
        cum = jnp.dot(lower, log_all[now], precision=EXACT, preferred_element_type=jnp.float32)
        cum_flat = jnp.dot(
            log_flat[:, now], upper, precision=EXACT, preferred_element_type=jnp.float32
        )
        step_row = step_flat[:, now]
        for group in range(groups):
            cols = slice(group * span, (group + 1) * span)
            x_now = silu(taps(x_pad, x_taps, at, cols))
            x_half = x_now.astype(jnp.bfloat16)
            b_now = bc_conv[now, group * STATE : (group + 1) * STATE]
            c_now = bc_conv[now, wide + group * STATE : wide + (group + 1) * STATE]
            spread = (
                lax.broadcasted_iota(jnp.int32, (heads, span), 0)
                == group * (span // HEAD_DIM)
                + lax.broadcasted_iota(jnp.int32, (heads, span), 1) // HEAD_DIM
            ).astype(jnp.float32)
            cum_wide = jnp.dot(cum, spread, precision=EXACT, preferred_element_type=jnp.float32)
            step_wide = jnp.dot(
                step_all[now], spread, precision=EXACT, preferred_element_type=jnp.float32
            )
            grown[now, cols] = jnp.exp(cum_wide)
            end = cum_wide[BLOCK - 1 : BLOCK]
            ends[at : at + 1, cols] = end
            scaled = (x_half.astype(jnp.float32) * jnp.exp(end - cum_wide) * step_wide).astype(
                jnp.bfloat16
            )
            b_flat = jnp.transpose(b_now.astype(jnp.float32)).astype(jnp.bfloat16)
            local_in[at, :, cols] = state[:, cols]
            state[:, cols] = state[:, cols] * jnp.exp(end) + jnp.dot(
                b_flat, scaled, preferred_element_type=jnp.float32
            )
            scores = jnp.dot(c_now, b_flat, preferred_element_type=jnp.float32)
            for pair in range(span // (2 * HEAD_DIM)):
                lanes = slice(pair * 2 * HEAD_DIM, (pair + 1) * 2 * HEAD_DIM)
                both = []
                for side in range(2):
                    head = group * (span // HEAD_DIM) + 2 * pair + side
                    gap = cum[:, head : head + 1] - cum_flat[head : head + 1]
                    decay = jnp.exp(jnp.where(causal, gap, -1e30))
                    weights = (scores * decay * step_row[head : head + 1]).astype(jnp.bfloat16)
                    both.append(
                        jnp.dot(weights, x_half[:, lanes], preferred_element_type=jnp.float32)
                    )
                here = group * span + pair * 2 * HEAD_DIM
                within[now, here : here + 2 * HEAD_DIM] = jnp.where(first_half, both[0], both[1])
            yield
    total_log = ends[0:1]
    for at in range(1, blocks):
        total_log = total_log + ends[at : at + 1]
    far_state[sp_size] = state[...].astype(jnp.bfloat16)
    far_log[sp_size] = jnp.broadcast_to(total_log, far_log.shape[1:])

    def letters(far):
        return [
            pltpu.make_async_remote_copy(
                src_ref=buffer.at[sp_size],
                dst_ref=buffer.at[far - 1],
                send_sem=sends.at[far - 1, kind],
                recv_sem=arrivals.at[far - 1, kind],
                device_id={"sp": sp_me + far},
                device_id_type=MESH_IDS,
            )
            for kind, buffer in enumerate((far_state, far_log))
        ]

    for far in range(1, sp_size):

        @pl.when(sp_me + far < sp_size)
        def _(far=far):
            for letter in letters(far):
                letter.start()

    yield
    place = sp_me * rows
    for group in range(pool_weight.shape[0]):
        cols = slice(group * POOL_GROUP, (group + 1) * POOL_GROUP)
        window = reach[:, cols]
        for at in range(blocks):
            now = slice(at * BLOCK, (at + 1) * BLOCK)
            running = None
            for back in range(tail):
                begin = at * BLOCK + tail - back
                term = pool_pad[begin : begin + BLOCK, cols] * jnp.where(back < window, 1.0, 0.0)
                running = term if running is None else running + term
            position = (
                place + at * BLOCK + lax.broadcasted_iota(jnp.int32, (BLOCK, POOL_GROUP), 0)
            ).astype(jnp.float32)
            pooled = running / jnp.minimum(position + 1.0, window) - pool_in[now, cols].astype(
                jnp.float32
            )
            mixed = jnp.dot(
                pooled.astype(jnp.bfloat16), pool_weight[group], preferred_element_type=jnp.float32
            )
            out = inner + group * POOL_GROUP
            channels[now, out : out + POOL_GROUP] = (
                mixed * pool_scale[:, cols].astype(jnp.float32)
            ).astype(jnp.bfloat16)
        yield
    before[...] = jnp.zeros_like(before)
    for far in range(sp_size - 1, 0, -1):

        @pl.when(sp_me - far >= 0)
        def _(far=far):
            for letter in letters(far):
                letter.wait_recv()
            before[...] = before[...] * jnp.exp(far_log[far - 1][0:1]) + far_state[far - 1].astype(
                jnp.float32
            )

    yield
    prefix = jnp.zeros_like(total_log)
    for at in range(blocks):
        now = slice(at * BLOCK, (at + 1) * BLOCK)
        for group in range(groups):
            cols = slice(group * span, (group + 1) * span)
            entering = local_in[at, :, cols] + jnp.exp(prefix[:, cols]) * before[:, cols]
            c_now = bc_conv[now, wide + group * STATE : wide + (group + 1) * STATE]
            carried = jnp.dot(
                c_now, entering.astype(jnp.bfloat16), preferred_element_type=jnp.float32
            )
            mixed = (within[now, cols] + carried * grown[now, cols]) * silu(
                gate[now, cols].astype(jnp.float32)
            )
            root = lax.rsqrt(jnp.mean(mixed * mixed, axis=1, keepdims=True) + eps)
            channels[now, cols] = (mixed * root * gain[:, cols].astype(jnp.float32)).astype(
                jnp.bfloat16
            )
        prefix = prefix + ends[at : at + 1]
        yield
    for far in range(1, sp_size):

        @pl.when(sp_me + far < sp_size)
        def _(far=far):
            for letter in letters(far):
                letter.wait_send()


def whole_kernel(sp_size, fs_size, tail, own, *refs):
    inputs, (whole, channels), scratch = refs[:18], refs[18:20], refs[20:]
    sends, arrivals, local_sem, letter_sends, letter_arrivals = scratch[:5]
    gather = Gather(own, whole, sends, arrivals, sp_size, fs_size)
    gather.barrier()
    at = (gather.sp_me * fs_size + gather.fs_at(0)) * gather.width
    mine = pltpu.make_async_copy(
        own, whole.at[:, pl.ds(pl.multiple_of(at, gather.width), gather.width)], local_sem
    )
    mine.start()
    moves = gather.run()
    work = mixers(
        (sp_size, tail), (*inputs, channels, *scratch[5:]), (letter_sends, letter_arrivals)
    )
    next(moves, None)
    for _ in work:
        next(moves, None)
    for _ in moves:
        pass
    mine.wait()
    gather.finish()


def mixed_and_gathered(own, inputs, tail):
    sp_size, fs_size = lax.axis_size("sp"), lax.axis_size("fs")
    rows, width = own.shape
    x_in, bc_in, pool_in = inputs[0], inputs[2], inputs[13]
    tok_rows, inner = x_in.shape
    blocks = tok_rows // BLOCK
    hops = hop_count(sp_size, fs_size)
    vmem = pl.BlockSpec(memory_space=pltpu.VMEM)
    return pl.pallas_call(
        functools.partial(whole_kernel, sp_size, fs_size, tail),
        out_shape=(
            jax.ShapeDtypeStruct((rows, width * sp_size * fs_size), own.dtype),
            jax.ShapeDtypeStruct((tok_rows, inner + pool_in.shape[1]), jnp.bfloat16),
        ),
        in_specs=[vmem] * (1 + len(inputs)),
        out_specs=(vmem, vmem),
        scratch_shapes=[
            pltpu.SemaphoreType.DMA((hops,)),
            pltpu.SemaphoreType.DMA((hops,)),
            pltpu.SemaphoreType.DMA,
            pltpu.SemaphoreType.DMA((sp_size, 2)),
            pltpu.SemaphoreType.DMA((sp_size, 2)),
            pltpu.VMEM((tail + tok_rows, inner), jnp.float32),
            pltpu.VMEM((tail + tok_rows, bc_in.shape[1]), jnp.float32),
            pltpu.VMEM((tail + tok_rows, pool_in.shape[1]), jnp.float32),
            pltpu.VMEM((8, 128), jnp.bfloat16),
            pltpu.VMEM((tok_rows, bc_in.shape[1]), jnp.bfloat16),
            pltpu.VMEM((tok_rows, inner), jnp.float32),
            pltpu.VMEM((tok_rows, inner), jnp.float32),
            pltpu.VMEM((blocks, STATE, inner), jnp.float32),
            pltpu.VMEM((STATE, inner), jnp.float32),
            pltpu.VMEM((-(-blocks // 8) * 8, inner), jnp.float32),
            pltpu.VMEM((STATE, inner), jnp.float32),
            pltpu.VMEM((sp_size + 1, STATE, inner), jnp.bfloat16),
            pltpu.VMEM((sp_size + 1, 8, inner), jnp.float32),
        ],
        compiler_params=pltpu.CompilerParams(
            collective_id=0, has_side_effects=True, vmem_limit_bytes=48 * 2**20
        ),
        name="mega_mixers",
    )(own, *inputs)


def causal_taps(input_rows, prior_rows, tap_weights, offset_bias):
    padded = jnp.concatenate([prior_rows, input_rows], axis=0).astype(jnp.float32)
    tok_rows = input_rows.shape[0]
    running = jnp.zeros(input_rows.shape, jnp.float32) + offset_bias
    for tap_index in range(tap_weights.shape[0]):
        running = (
            running
            + tap_weights[tap_index].astype(jnp.float32) * padded[tap_index : tap_index + tok_rows]
        )
    return jax.nn.silu(running).astype(jnp.bfloat16)


def pool_mix(input_rows, prior_rows, positions, group_ids, local_weight, local_scale):
    tail_rows = prior_rows.shape[0]
    tok_rows = input_rows.shape[0]
    padded = jnp.concatenate([prior_rows, input_rows], axis=0).astype(jnp.float32)
    window_reach = jnp.left_shift(jnp.int32(2), group_ids)
    running = jnp.zeros(input_rows.shape, jnp.float32)
    for offset_back in range(tail_rows + 1):
        start_row = tail_rows - offset_back
        running = running + padded[start_row : start_row + tok_rows] * (
            offset_back < window_reach
        ).astype(jnp.float32)
    window_count = jnp.minimum(positions[:, None] + 1.0, window_reach.astype(jnp.float32)[None, :])
    pooled = (running / window_count - input_rows.astype(jnp.float32)).astype(jnp.bfloat16)
    grouped = pooled.reshape(tok_rows, local_weight.shape[0], local_weight.shape[1])
    mixed = jnp.einsum("lgc,gcd->lgd", grouped, local_weight, preferred_element_type=jnp.float32)
    return (mixed.reshape(input_rows.shape) * local_scale.astype(jnp.float32)).astype(jnp.bfloat16)


def join_states(earlier, later_part):
    return (
        earlier[0] + later_part[0],
        earlier[1] * jnp.exp(later_part[0])[..., None, None] + later_part[1],
    )


def body(
    statespace_input,
    output_gate_input,
    state_input_projection,
    state_output_projection,
    step_size_input,
    added_log_decay,
    logarithm_rates,
    head_channel_taps,
    input_projection_taps,
    output_projection_taps,
    input_projection_bias,
    group_norm_gain,
    pooling_input,
    pooling_group_weight,
    pooling_channel_scale,
    statespace_output_weight,
    pooling_output_weight,
    output_norm_gain,
):
    core_index = lax.axis_index("tp")
    core_count = lax.axis_size("tp")
    seq_index = lax.axis_index("sp")
    head_channel_rows = statespace_input[0]
    output_gate_rows = output_gate_input[0]
    input_projection_rows = state_input_projection[0]
    output_projection_rows = state_output_projection[0]
    step_size_rows = step_size_input[0]
    decay_spikes = added_log_decay[0]
    pooling_rows = pooling_input[0]
    tok_rows = head_channel_rows.shape[0]
    inner_local = head_channel_rows.shape[1]
    heads_local = step_size_rows.shape[1]
    state_local = input_projection_rows.shape[1]
    pool_local = pooling_rows.shape[1]
    groups_local = state_local // STATE
    per_group = heads_local // groups_local
    groups_pool = pool_local // POOL_GROUP
    pool_tail = 2**POOL_GROUPS - 1
    conv_tail = CONV - 1
    own_columns = jnp.concatenate([statespace_output_weight, pooling_output_weight], axis=0)
    tails = jnp.concatenate(
        [
            jnp.pad(rows[tok_rows - tail :], ((pool_tail - tail, 0), (0, 0)))
            for rows, tail in (
                (head_channel_rows, conv_tail),
                (input_projection_rows, conv_tail),
                (output_projection_rows, conv_tail),
                (pooling_rows, pool_tail),
            )
        ],
        axis=1,
    )
    prior = passed_along(tails, "sp", 1)
    widths = (inner_local, state_local, state_local, pool_local)
    prior_x, prior_b, prior_c, prior_pool = (
        prior[pool_tail - tail :, sum(widths[:at]) : sum(widths[: at + 1])]
        for at, tail in enumerate((conv_tail, conv_tail, conv_tail, pool_tail))
    )
    taps_x = lax.dynamic_slice_in_dim(head_channel_taps, core_index * inner_local, inner_local, 1)
    taps_b = lax.dynamic_slice_in_dim(
        input_projection_taps, core_index * state_local, state_local, 1
    )
    taps_c = lax.dynamic_slice_in_dim(
        output_projection_taps, core_index * state_local, state_local, 1
    )
    bias_b = lax.dynamic_slice_in_dim(
        input_projection_bias, core_index * state_local, state_local, 0
    )
    gain_ssd = lax.dynamic_slice_in_dim(group_norm_gain, core_index * inner_local, inner_local, 0)
    head_decay_rates = jnp.exp(
        lax.dynamic_slice_in_dim(logarithm_rates, core_index * heads_local, heads_local, 0)
    )
    gain_pool = lax.dynamic_slice_in_dim(
        pooling_channel_scale, core_index * pool_local, pool_local, 0
    )
    weight_pool = lax.dynamic_slice_in_dim(
        pooling_group_weight, core_index * groups_pool, groups_pool, 0
    )
    tail = pool_tail + 1
    local_width = own_columns.shape[1]
    narrow = local_width % 128 != 0 or lax.axis_size("sp") > 8
    if narrow:
        whole_columns = lax.all_gather(own_columns, ("sp", "fs"), axis=1, tiled=True)
        x_conv = causal_taps(head_channel_rows, prior_x, taps_x, 0.0)
        b_conv = causal_taps(input_projection_rows, prior_b, taps_b, bias_b.astype(jnp.float32))
        c_conv = causal_taps(output_projection_rows, prior_c, taps_c, 0.0)
        blocks = tok_rows // BLOCK
        discrete_step_size = jax.nn.softplus(step_size_rows.astype(jnp.float32))
        logarithm_decay = -discrete_step_size * head_decay_rates + decay_spikes
        cumulative_decay = jnp.cumsum(
            logarithm_decay.reshape(blocks, BLOCK, groups_local, per_group), axis=1
        )
        cum_t = cumulative_decay.transpose(0, 2, 3, 1)
        step_t = discrete_step_size.reshape(blocks, BLOCK, groups_local, per_group).transpose(
            0, 2, 3, 1
        )
        heads_x = x_conv.reshape(blocks, BLOCK, groups_local, per_group, HEAD_DIM)
        group_b = b_conv.reshape(blocks, BLOCK, groups_local, STATE)
        group_c = c_conv.reshape(blocks, BLOCK, groups_local, STATE)
        scores = jnp.einsum("ktgn,kugn->kgtu", group_c, group_b, preferred_element_type=jnp.float32)
        causal = jnp.arange(BLOCK)[:, None] >= jnp.arange(BLOCK)[None, :]
        decay_gap = cum_t[..., :, None] - cum_t[..., None, :]
        decay_factor = jnp.where(causal, jnp.exp(jnp.where(causal, decay_gap, 0.0)), 0.0)
        weights = (scores[:, :, None] * decay_factor * step_t[..., None, :]).astype(jnp.bfloat16)
        within = jnp.einsum("kgetu,kugep->ktgep", weights, heads_x, preferred_element_type=jnp.float32)
        block_end = cum_t[..., -1]
        end_weight = jnp.exp(block_end[..., None] - cum_t) * step_t
        scaled_x = (heads_x * end_weight.transpose(0, 3, 1, 2)[..., None]).astype(jnp.bfloat16)
        block_state = jnp.einsum(
            "kugep,kugn->kgepn", scaled_x, group_b, preferred_element_type=jnp.float32
        )

        def local_chain(state_now, current_inputs):
            piece_state, piece_fall = current_inputs
            return (state_now * jnp.exp(piece_fall)[..., None, None] + piece_state, state_now)

        final_state, local_entering = lax.scan(
            local_chain, jnp.zeros(block_state.shape[1:], jnp.float32), (block_state, block_end)
        )
        log_total = jnp.sum(block_end, axis=0)
        prefix_log = jnp.cumsum(block_end, axis=0) - block_end
        log_before, state_before = entering_2(
            (log_total, final_state),
            "sp",
            join_states,
            (jnp.zeros_like(log_total), jnp.zeros_like(final_state)),
        )
        entering = (local_entering + jnp.exp(prefix_log)[..., None, None] * state_before[None]).astype(
            jnp.bfloat16
        )
        carried_out = jnp.einsum(
            "ktgn,kgepn->ktgep", group_c, entering, preferred_element_type=jnp.float32
        )
        carried_out = carried_out * jnp.exp(cumulative_decay)[..., None]
        mixed_ssd = (within + carried_out).reshape(tok_rows, inner_local) * jax.nn.silu(
            output_gate_rows.astype(jnp.float32)
        )
        grouped = mixed_ssd.reshape(tok_rows, groups_local, inner_local // groups_local)
        normed = grouped * lax.rsqrt(jnp.mean(grouped * grouped, axis=-1, keepdims=True) + eps)
        ssd_out = (normed.reshape(tok_rows, inner_local) * gain_ssd.astype(jnp.float32)).astype(
            jnp.bfloat16
        )
        positions = (seq_index * tok_rows + jnp.arange(tok_rows, dtype=jnp.int32)).astype(jnp.float32)
        group_ids = core_index * groups_pool + jnp.arange(pool_local, dtype=jnp.int32) // POOL_GROUP
        pool_out = pool_mix(pooling_rows, prior_pool, positions, group_ids, weight_pool, gain_pool)
        channels = jnp.concatenate([ssd_out, pool_out], axis=1)
    else:
        rates = lax.dynamic_slice_in_dim(logarithm_rates, core_index * heads_local, heads_local, 0)
        group_ids = core_index * groups_pool + jnp.arange(pool_local, dtype=jnp.int32) // POOL_GROUP
        reach = jnp.left_shift(jnp.int32(2), group_ids).astype(jnp.float32)
        bias = jnp.concatenate([bias_b, jnp.zeros_like(bias_b)])
        whole_columns, channels = mixed_and_gathered(
            own_columns,
            (
                head_channel_rows,
                output_gate_rows,
                jnp.concatenate([input_projection_rows, output_projection_rows], axis=1),
                step_size_rows,
                step_size_rows.T,
                decay_spikes,
                decay_spikes.T,
                rates[None],
                rates[:, None],
                taps_x,
                jnp.concatenate([taps_b, taps_c], axis=1),
                bias[None],
                gain_ssd[None],
                pooling_rows,
                weight_pool,
                gain_pool[None],
                reach[None],
                jnp.pad(prior, ((tail - pool_tail, 0), (0, 0))),
            ),
            tail,
        )
    half_width = D // core_count
    gain_out = lax.dynamic_slice_in_dim(
        output_norm_gain, core_index * half_width, half_width, 0
    ).astype(jnp.float32)
    partial = jnp.dot(channels, whole_columns, preferred_element_type=jnp.float32).astype(
        jnp.bfloat16
    )
    own_half = lax.dynamic_slice_in_dim(partial, core_index * half_width, half_width, 1).astype(
        jnp.float32
    )
    for hop in range(1, core_count):
        target = lax.rem(core_index + hop, core_count)
        leaving = lax.dynamic_slice_in_dim(partial, target * half_width, half_width, 1)
        route = [(i, (i + hop) % core_count) for i in range(core_count)]
        own_half = own_half + lax.ppermute(leaving, "tp", route).astype(jnp.float32)
    row_squares = lax.psum(jnp.sum(own_half * own_half, axis=1), "tp")
    result = own_half * lax.rsqrt(row_squares / D + eps)[:, None] * gain_out
    return result.astype(jnp.bfloat16)[None]


def solution(mesh):
    in_specs = (
        P("fs", "sp", "tp"),
        P("fs", "sp", "tp"),
        P("fs", "sp", "tp"),
        P("fs", "sp", "tp"),
        P("fs", "sp", "tp"),
        P("fs", "sp", "tp"),
        P(),
        P(),
        P(),
        P(),
        P(),
        P(),
        P("fs", "sp", "tp"),
        P(),
        P(),
        P("tp", ("sp", "fs")),
        P("tp", ("sp", "fs")),
        P(),
    )
    out_specs = P("fs", "sp", "tp")
    return jax.shard_map(body, mesh=mesh, in_specs=in_specs, out_specs=out_specs, check_vma=False)
```

profile of v0, /device:TPU:25, one launch (start us, length us, event | category | flops | bytes accessed | tf_op | source)
XLA Modules:
  0.0 157.5 jit_solution(12189237874491325144)
XLA Ops:
  0.0 0.0 copy-start
  0.0 0.0 copy-start.4
  0.0 0.0 copy-start.5
  0.0 0.8 slice_bitcast_fusion
  0.9 0.7 slice_bitcast_fusion.1
  1.6 0.7 slice_bitcast_fusion.2
  2.3 0.6 fusion.7
  3.0 1.3 collective-permute-start
  4.3 0.7 dynamic-slice_bitcast_fusion
  5.0 0.1 copy.21.refs_8_
  5.1 0.7 constant_dynamic-slice_fusion.4.refs_9_
  5.8 0.7 dynamic_slice.38
  6.5 0.8 dynamic_slice.37
  7.2 0.8 dynamic_slice.40
  8.0 0.9 copy.20.refs_5_
  8.9 0.8 copy.19.refs_3_
  9.7 0.7 constant_dynamic-slice_fusion.2
  10.5 1.2 pad_maximum_fusion.own
  11.6 1.1 pad_maximum_fusion.1.refs_2_
  12.7 0.0 collective-permute-done
  12.7 0.9 pad.19.refs_17_
  13.6 0.0 copy-start.2
  13.7 1.1 copy-done.2
  14.8 116.8 %mega_mixers.1 = (bf16[1536,4096]{1,0:T(8,128)(2,1)}, bf16[384,1536]{1,0:T(8,128)(2,1)S(1)}) custom-call(bf16[1536,256]{1,0:T(8,128)(2,1)S(1)} %pad_maximum_fusion.own, bf16[384,1024]{1,0:T(8,128)(2,1)S(1)} %bitcast.27, bf16[384,1024]{1,0:T(8,128)(2,1)S(1)} %bitcast.28, bf16[384,512]{1,0:T(8,128)(2,1)S(1)} %pad_maximum_fusion.1.refs_2_, ...), custom_call_target="tpu_custom_call" | custom-call | tf_op jit(solution)/shard_map/mega_mixers/pallas_call | solution.py:447
  131.6 9.8 %convolution_convert_fusion = bf16[384,4096]{1,0:T(8,128)(2,1)S(1)} fusion(bf16[384,1536]{1,0:T(8,128)(2,1)S(1)} %get-tuple-element.7, bf16[1536,4096]{1,0:T(8,128)(2,1)} %get-tuple-element.8), kind=kOutput, calls=%fused_computation | convolution fusion | flops 4833411072 | bytes 16908288 | tf_op jit(solution)/shard_map/dot_general | solution.py:699
  141.4 1.6 %copy-done.6 = bf16[384,4096]{1,0:T(8,128)(2,1)} copy-done((bf16[384,4096]{1,0:T(8,128)(2,1)}, bf16[384,4096]{1,0:T(8,128)(2,1)S(1)}, u32[]{:S(2)}) %copy-start.6) | copy-done | bytes 3145752
  143.1 1.3 constant_dynamic-slice_fusion
  144.4 2.0 %collective-permute-start.1 = (bf16[384,2048]{1,0:T(8,128)(2,1)}, bf16[384,2048]{1,0:T(8,128)(2,1)S(1)}, u32[]{:S(2)}, u32[]{:S(2)}) collective-permute-start(bf16[384,2048]{1,0:T(8,128)(2,1)} %constant_dynamic-slice_fusion), channel_id=1, source_target_pairs={{0,1},{1,0},{2,3},{3,2},{4,5},{5,4},{6,7},{7,6},{8,9},{9,8},{10,11... | collective-permute-start | bytes 4718600 | tf_op jit(solution)/shard_map/ppermute | solution.py:709
  146.4 3.2 %collective-permute-done.1 = bf16[384,2048]{1,0:T(8,128)(2,1)S(1)} collective-permute-done((bf16[384,2048]{1,0:T(8,128)(2,1)}, bf16[384,2048]{1,0:T(8,128)(2,1)S(1)}, u32[]{:S(2)}, u32[]{:S(2)}) %collective-permute-start.1) | collective-permute-done | bytes 1572896 | tf_op jit(solution)/shard_map/ppermute | solution.py:709
  149.7 2.0 %multiply_reduce_fusion = f32[384]{0:T(512)S(1)} fusion(bf16[384,2048]{1,0:T(8,128)(2,1)S(1)} %collective-permute-done.1, bf16[384,4096]{1,0:T(8,128)(2,1)} %copy-done.6, s32[]{:T(128)S(6)} %select_n.43), kind=kLoop, calls=%fused_computation.2 | loop fusion | flops 3931776 | bytes 3147268 | tf_op jit(solution)/shard_map/reduce_sum | solution.py:710
  151.7 2.5 %psum.7 = f32[384]{0:T(512)S(1)} all-reduce(f32[384]{0:T(512)S(1)} %multiply_reduce_fusion), channel_id=1, replica_groups=mesh['sp'=4,'fs'=4,'tp'=2] {'tp'}, use_global_device_ids=true, to_apply=%region_1.2 | all-reduce | flops 384 | bytes 3072 | tf_op jit(solution)/shard_map/psum | solution.py:710
  154.2 3.4 %fusion = bf16[1,384,2048]{2,1,0:T(8,128)(2,1)} fusion(bf16[384,2048]{1,0:T(8,128)(2,1)S(1)} %collective-permute-done.1, f32[2048]{0:T(1024)S(1)} %dynamic-slice_convert_fusion, f32[384]{0:T(512)S(1)} %add_rsqrt_fusion, bf16[384,4096]{1,0:T(8,128)(2,1)} %copy-done.6, s32[]{:T(128)S(6)} %select_n.43), kind=kLoop, calls=%fused_computation.4 | loop fusion | flops 4718592 | bytes 4728324 | tf_op jit(solution)/shard_map/broadcast_in_dim | solution.py:712
  (19 shorter events, 0.1 us)
Async XLA Ops:
  0.0 10.4 %copy-start = (bf16[4,256,256]{2,1,0:T(8,128)(2,1)S(1)}, bf16[4,256,256]{2,1,0:T(8,128)(2,1)}, u32[]{:S(2)}) copy-start(bf16[4,256,256]{2,1,0:T(8,128)(2,1)} %param.31) | copy-start | bytes 1572868
  0.0 13.6 %copy-start.3 = (bf16[1,384,512]{2,1,0:T(8,128)(2,1)S(1)}, bf16[1,384,512]{2,1,0:T(8,128)(2,1)}, u32[]{:S(2)}) copy-start(bf16[1,384,512]{2,1,0:T(8,128)(2,1)} %param.30) | copy-start | bytes 1179652
  0.0 13.6 %copy-start.1 = (bf16[1,384,1024]{2,1,0:T(8,128)(2,1)S(1)}, bf16[1,384,1024]{2,1,0:T(8,128)(2,1)}, u32[]{:S(2)}) copy-start(bf16[1,384,1024]{2,1,0:T(8,128)(2,1)} %param.18) | copy-start | bytes 2359300
  0.0 13.6 %copy-start.4 = (f32[1,384,16]{1,2,0:T(8,128)S(1)}, f32[1,384,16]{1,2,0:T(8,128)}, u32[]{:S(2)}) copy-start(f32[1,384,16]{1,2,0:T(8,128)} %param.23) | copy-start | bytes 73732
  0.0 13.6 %copy-start.5 = (bf16[1,384,16]{1,2,0:T(8,128)(2,1)S(1)}, bf16[1,384,16]{1,2,0:T(8,128)(2,1)}, u32[]{:S(2)}) copy-start(bf16[1,384,16]{1,2,0:T(8,128)(2,1)} %param.22) | copy-start | bytes 36868
  3.0 9.8 %collective-permute-start = (bf16[15,2048]{1,0:T(8,128)(2,1)}, bf16[15,2048]{1,0:T(8,128)(2,1)}, u32[]{:S(2)}, u32[]{:S(2)}) collective-permute-start(bf16[15,2048]{1,0:T(8,128)(2,1)} %fusion.7), channel_id=1, source_target_pairs={{0,8},{8,16},{16,24},{1,9},{9,17},{17,25},{2,10},{10,18},{18,26},{... | collective-permute-start | bytes 184328 | tf_op jit(solution)/shard_map/ppermute | solution.py:25
  13.6 1.1 copy-start.2
  141.4 1.6 %copy-start.6 = (bf16[384,4096]{1,0:T(8,128)(2,1)}, bf16[384,4096]{1,0:T(8,128)(2,1)S(1)}, u32[]{:S(2)}) copy-start(bf16[384,4096]{1,0:T(8,128)(2,1)S(1)} %convolution_convert_fusion) | copy-start | bytes 9437188
  143.1 3.4 %copy-start.7 = (bf16[4096]{0:T(1024)(128)(2,1)S(1)}, bf16[4096]{0:T(1024)(128)(2,1)}, u32[]{:S(2)}) copy-start(bf16[4096]{0:T(1024)(128)(2,1)} %param.35) | copy-start | bytes 24580
  144.4 5.3 %collective-permute-start.1 = (bf16[384,2048]{1,0:T(8,128)(2,1)}, bf16[384,2048]{1,0:T(8,128)(2,1)S(1)}, u32[]{:S(2)}, u32[]{:S(2)}) collective-permute-start(bf16[384,2048]{1,0:T(8,128)(2,1)} %constant_dynamic-slice_fusion), channel_id=1, source_target_pairs={{0,1},{1,0},{2,3},{3,2},{4,5},{5,4},{6,7},{7,6},{8,9},{9,8},{10,11... | collective-permute-start | bytes 4718600 | tf_op jit(solution)/shard_map/ppermute | solution.py:709
where the time goes:
time: 158 us
  Pallas kernels  117 us (74%)
  local copies, waits for them, and re-layouts  13.4 us (8%)
  matrix products  9.84 us (6%)
  other arithmetic  8.26 us (5%)
  starting transfers between devices  3.33 us (2%)
  waiting for transfers between devices  3.24 us (2%)
  blocking collectives  2.49 us (2%)
    pallas_call x1, Pallas kernels, mixed_and_gathered(): pl.pallas_call(functools.partial(whole_kernel, sp_size, fs_size, tail), o...  117 us
    dot_general x1, matrix products, body(): jnp.dot(channels, whole_columns, preferred_element_type=jnp.float32)  9.84 us
    broadcast_in_dim x1, other arithmetic, body(): return result.astype(jnp.bfloat16)[None]  3.36 us
    ppermute x1, waiting for transfers between devices, body(): own_half = own_half + lax.ppermute(leaving, 'tp', route).astype(jnp.float32)  3.24 us
  transfers between devices with their start and end apart: 2, of which 1 were waited for; matrix products, arithmetic and copies ran while one was open for 5% of the time, Pallas kernels for 0%

commit v1 on v0

v1 whole, which is shorter than its diff:
```python
import functools

import jax
import jax.numpy as jnp
from jax import lax
from jax.experimental import pallas as pl
from jax.experimental.pallas import tpu as pltpu
from jax.sharding import PartitionSpec as P

D = 4096
HEAD_DIM = 64
STATE = 128
CONV = 4
BLOCK = 128
POOL_GROUPS = 4
POOL_GROUP = 256


eps = 1e-06


def passed_along(block, axis, distance):
    devices = range(lax.axis_size(axis))
    route = [(i - distance, i) for i in devices if i - distance in devices]
    return lax.ppermute(block, axis, route)


def entering_2(array, axis, join, neutral):
    place = lax.axis_index(axis)
    gathered = jax.tree.map(
        lambda a, kind: lax.all_gather(a.astype(kind), axis), array, (jnp.bfloat16, jnp.bfloat16)
    )
    state = jax.tree.map(lambda a, e: jnp.zeros_like(a) + jnp.asarray(e, a.dtype), array, neutral)

    def one(lap, state):
        return join(
            state,
            jax.tree.map(
                lambda a, own: lax.dynamic_index_in_dim(a, lap, 0, False).astype(own.dtype),
                gathered,
                array,
            ),
        )

    return lax.fori_loop(0, place, one, state)


MESH_IDS = pl.DeviceIdType.MESH
EXACT = lax.Precision.HIGHEST
CHUNKS = 6
PAUSE = 0


class Links:
    def __init__(self, sp_size, fs_size):
        self.n = sp_size
        self.z = lax.axis_index("sp")
        self.fs = lax.axis_index("fs")
        self.core = lax.axis_index("tp")
        self.x = lax.rem(self.fs, 2)
        self.y = self.fs // 2
        self.beside = {"fs": self.fs + 1 - 2 * self.x}
        self.across = {"fs": self.fs + 2 - 4 * self.y}
        self.sibling = {"tp": 1 - self.core}

    def barrier(self):
        barrier = pltpu.get_barrier_semaphore()
        near = [{"sp": lax.rem(self.z + far, self.n)} for far in (1, self.n - 1)]
        for other in (*near, self.beside, self.across, self.sibling):
            pl.semaphore_signal(barrier, inc=1, device_id=other, device_id_type=MESH_IDS)
        pl.semaphore_wait(barrier, len(near) + 3)

    def within(self, place):
        return jnp.logical_and(place >= 0, place < self.n)

    def nearest(self, turn):
        if turn == 0:
            return self.z
        low, high = self.z, self.n - 1 - self.z
        small = jnp.minimum(low, high)
        both = turn <= 2 * small
        far = jnp.where(both, (turn + 1) // 2, turn - small)
        sign = jnp.where(both, 1 - 2 * (turn % 2), jnp.where(high > low, 1, -1))
        return self.z + sign * far


def remote(src, dst, sends, arrivals, spot, device):
    return pltpu.make_async_remote_copy(
        src_ref=src,
        dst_ref=dst,
        send_sem=sends.at[spot],
        recv_sem=arrivals.at[spot],
        device_id=device,
        device_id_type=MESH_IDS,
    )


class Weights:
    def __init__(self, links, whole, width, z_sems, y_sems):
        self.links, self.whole, self.width = links, whole, width
        self.z_sems, self.y_sems = z_sems, y_sems
        self.rows = whole.shape[0] // CHUNKS
        self.direct = range(CHUNKS - 1)
        self.turned = (CHUNKS - 1,)
        self.sent = []

    def region(self, chunk, z, y):
        at = pl.multiple_of((z * 2 + y) * self.width, self.width)
        return self.whole.at[pl.ds(chunk * self.rows, self.rows), pl.ds(at, self.width)]

    def along(self, chunk, step, way, side, arriving):
        links = self.links
        origin = links.z - way * (step if arriving else step - 1)
        y = links.y if side == 0 else 1 - links.y
        spot = ((chunk * (links.n - 1) + step - 1) * 2 + (way < 0)) * 2 + side
        place = self.region(chunk, jnp.clip(origin, 0, links.n - 1), y)
        copy = remote(place, place, *self.z_sems, spot, {"sp": links.z + way})
        far = links.z if arriving else links.z + way
        return copy, jnp.logical_and(links.within(origin), links.within(far))

    def over(self, chunk, offset, arriving):
        links = self.links
        y = 1 - links.y if arriving else links.y
        origin = links.z + offset
        place = self.region(chunk, jnp.clip(origin, 0, links.n - 1), y)
        spot = chunk * (2 * links.n - 1) + offset + links.n - 1
        copy = remote(place, place, *self.y_sems, spot, links.across)
        return copy, links.within(origin)

    def go(self, kind, *key):
        copy, here = kind(*key, False)
        self.sent.append((kind, key))
        pl.when(here)(copy.start)

    def take(self, kind, *key):
        copy, here = kind(*key, True)
        pl.when(here)(copy.wait_recv)

    def pass_on(self, chunk, step, way, side):
        if step < self.links.n:
            self.go(self.along, chunk, step, way, side)

    def begin(self):
        for chunk in self.turned:
            self.go(self.over, chunk, 0)
        for chunk in self.direct:
            for way in (1, -1):
                self.pass_on(chunk, 1, way, 0)
            self.go(self.over, chunk, 0)
        for chunk in self.turned:
            for way in (1, -1):
                self.pass_on(chunk, 1, way, 0)

    def turn(self):
        for chunk in self.turned:
            self.take(self.over, chunk, 0)
            for way in (1, -1):
                self.pass_on(chunk, 1, way, 1)

    def hop(self, step, chunk):
        for way in (1, -1):
            if chunk in self.turned:
                for side in (0, 1):
                    self.take(self.along, chunk, step, way, side)
                    self.pass_on(chunk, step + 1, way, side)
            else:
                self.take(self.along, chunk, step, way, 0)
                self.pass_on(chunk, step + 1, way, 0)
                self.go(self.over, chunk, -way * step)

    def settle(self, step):
        for chunk in self.direct:
            for offset in (0,) if step == 0 else (step, -step):
                self.take(self.over, chunk, offset)

    def finish(self):
        for kind, key in self.sent:
            copy, here = kind(*key, False)
            pl.when(here)(copy.wait_send)


def silu(rows):
    return rows / (1.0 + jnp.exp(-rows))


def softplus(rows):
    return jnp.maximum(rows, 0.0) + jnp.log(1.0 + jnp.exp(-jnp.abs(rows)))


def chosen(core, options):
    best = options[0]
    for at in range(1, len(options)):
        best = jnp.where(core == at, options[at], best)
    return best


def mixers(links, tail, cores, refs, sems):
    (x_in, gate, b_in, c_in, dt, added, rates, x_taps, b_taps, c_taps, bias, gain, pool_in,
     pool_weight, pool_scale, prior_x, prior_b, prior_c, prior_pool, x_pad, bc_pad, pool_pad,
     pool_two, pool_four, x_split, bc_conv, b_turned, cum_all, step_all, within, grown, local_in,
     state, before, carry_in, carry_out, channels, far_channels) = refs
    sends, arrivals = sems
    rows, inner = x_in.shape[1:]
    heads = dt.shape[2]
    wide = b_in.shape[2]
    pool = pool_in.shape[2]
    groups = wide // STATE
    span = inner // groups
    blocks = rows // BLOCK
    z, core = links.z, links.core
    lead = 8
    sources = ((x_in, prior_x), (b_in, prior_b), (c_in, prior_c), (pool_in, prior_pool))

    def tails(at):
        source, target = sources[at]
        return remote(
            source.at[0, pl.ds(rows - tail, tail)], target, sends, arrivals, at, {"sp": z + 1}
        )

    def chain(group):
        return remote(
            carry_out.at[group], carry_in.at[group], sends, arrivals, 4 + group, {"sp": z + 1}
        )

    def pool_letter():
        cols = pl.ds(inner, pool)
        return remote(
            channels.at[:, cols], far_channels.at[:, cols], sends, arrivals, 4 + groups, links.beside
        )

    def block_letter(at):
        place = (pl.ds(at * BLOCK, BLOCK), pl.ds(0, inner))
        return remote(
            channels.at[place], far_channels.at[place], sends, arrivals, 5 + groups + at, links.beside
        )

    follows = z + 1 < links.n

    @pl.when(follows)
    def _():
        for at in range(4):
            tails(at).start()

    yield
    x_pad[tail:] = x_in[0].astype(jnp.float32)
    bc_pad[tail:, 0:wide] = b_in[0].astype(jnp.float32)
    bc_pad[tail:, wide:] = c_in[0].astype(jnp.float32)
    pool_pad[0:lead] = jnp.zeros((lead, pool), jnp.float32)
    pool_pad[lead + tail :] = pool_in[0].astype(jnp.float32)
    cum_all[...] = jnp.zeros_like(cum_all)
    step_all[...] = jnp.zeros_like(step_all)
    steps = softplus(dt[0].astype(jnp.float32))
    step_all[:, 0:heads] = steps
    own_rates = chosen(core, [rates[:, c * heads : (c + 1) * heads] for c in range(cores)])
    logs = -steps * jnp.exp(own_rates) + added[0]
    down = lax.broadcasted_iota(jnp.int32, (BLOCK, BLOCK), 0)
    over = lax.broadcasted_iota(jnp.int32, (BLOCK, BLOCK), 1)
    causal = down >= over
    lower = causal.astype(jnp.float32)
    first_half = lax.broadcasted_iota(jnp.int32, (BLOCK, 2 * HEAD_DIM), 1) < HEAD_DIM

    def mine(ref, size):
        at = pl.multiple_of(core * size, size)
        return ref[:, pl.ds(at, size)].astype(jnp.float32)

    taps_x = mine(x_taps, inner)
    taps_bc = jnp.concatenate([mine(b_taps, wide), mine(c_taps, wide)], axis=1)
    bias_b = mine(bias, wide)
    bias_bc = jnp.concatenate([bias_b, jnp.zeros_like(bias_b)], axis=1)

    @pl.when(z == 0)
    def _():
        x_pad[0:tail] = jnp.zeros((tail, inner), jnp.float32)
        bc_pad[0:tail] = jnp.zeros((tail, 2 * wide), jnp.float32)
        pool_pad[lead : lead + tail] = jnp.zeros((tail, pool), jnp.float32)

    @pl.when(z > 0)
    def _():
        for at in range(4):
            tails(at).wait_recv()
        x_pad[0:tail] = prior_x[...].astype(jnp.float32)
        bc_pad[0:tail, 0:wide] = prior_b[...].astype(jnp.float32)
        bc_pad[0:tail, wide:] = prior_c[...].astype(jnp.float32)
        pool_pad[lead : lead + tail] = prior_pool[...].astype(jnp.float32)

    def taps(pad, weights, at, cols):
        total = None
        for tap in range(CONV):
            begin = at * BLOCK + tail - CONV + 1 + tap
            term = pad[begin : begin + BLOCK, cols] * weights[tap : tap + 1, cols]
            total = term if total is None else total + term
        return total

    def spread(narrow, head):
        shape = (BLOCK, 2 * HEAD_DIM)
        return jnp.where(
            first_half,
            jnp.broadcast_to(narrow[:, head : head + 1], shape),
            jnp.broadcast_to(narrow[:, head + 1 : head + 2], shape),
        )

    yield
    pairs = span // (2 * HEAD_DIM)
    ends = []
    state[...] = jnp.zeros_like(state)
    for at in range(blocks):
        now = slice(at * BLOCK, (at + 1) * BLOCK)
        bc_conv[now] = silu(taps(bc_pad, taps_bc, at, slice(0, 2 * wide)) + bias_bc).astype(
            jnp.bfloat16
        )
        cum = jnp.dot(lower, logs[now], precision=EXACT, preferred_element_type=jnp.float32)
        cum_all[now, 0:heads] = cum
        decayed = jnp.exp(cum)
        closing = jnp.exp(cum[BLOCK - 1 : BLOCK] - cum) * steps[now]
        ended = []
        for group in range(groups):
            cols = slice(group * span, (group + 1) * span)
            x_now = silu(taps(x_pad, taps_x, at, cols))
            b_now = bc_conv[now, group * STATE : (group + 1) * STATE]
            b_flat = jnp.transpose(b_now.astype(jnp.float32)).astype(jnp.bfloat16)
            b_turned[at * groups + group] = b_flat
            scaled = []
            for pair in range(pairs):
                head = group * (span // HEAD_DIM) + 2 * pair
                lanes = slice(pair * 2 * HEAD_DIM, (pair + 1) * 2 * HEAD_DIM)
                here = slice(head * HEAD_DIM, (head + 2) * HEAD_DIM)
                x_pair = x_now[:, lanes]
                x_split[at, 0:BLOCK, here] = jnp.where(first_half, x_pair, 0.0).astype(jnp.bfloat16)
                x_split[at, BLOCK : 2 * BLOCK, here] = jnp.where(first_half, 0.0, x_pair).astype(
                    jnp.bfloat16
                )
                x_half = x_pair.astype(jnp.bfloat16).astype(jnp.float32)
                scaled.append((x_half * spread(closing, head)).astype(jnp.bfloat16))
                grown[now, here] = spread(decayed, head)
            end = grown[(at + 1) * BLOCK - 1 : (at + 1) * BLOCK, cols]
            ended.append(end)
            local_in[at, :, cols] = state[:, cols]
            state[:, cols] = state[:, cols] * end + jnp.dot(
                b_flat, jnp.concatenate(scaled, axis=1), preferred_element_type=jnp.float32
            )
            yield
        ends.append(ended)

    def hand_on():
        @pl.when(z == 0)
        def _():
            before[...] = jnp.zeros_like(before)

        for group in range(groups):
            cols = slice(group * span, (group + 1) * span)

            @pl.when(z > 0)
            def _(group=group, cols=cols):
                chain(group).wait_recv()
                before[:, cols] = carry_in[group].astype(jnp.float32)

            @pl.when(follows)
            def _(group=group, cols=cols):
                falling = ends[0][group]
                for at in range(1, blocks):
                    falling = falling * ends[at][group]
                carry_out[group] = (before[:, cols] * falling + state[:, cols]).astype(jnp.bfloat16)
                chain(group).start()

    def chain_point(place, last=False):
        pl.when(z >= place if last else z == place)(hand_on)

    chain_point(0)
    yield
    place = z * rows
    position = (place + lax.broadcasted_iota(jnp.int32, (rows, 1), 0)).astype(jnp.float32) + 1.0
    pool_groups = pool // POOL_GROUP
    for group in range(pool_groups):
        cols = slice(group * POOL_GROUP, (group + 1) * POOL_GROUP)
        size = rows + tail
        two = pool_pad[lead:, cols] + pool_pad[lead - 1 : lead - 1 + size, cols]
        pool_two[0:lead] = jnp.zeros((lead, POOL_GROUP), jnp.float32)
        pool_two[lead:] = two
        four = two + pool_two[lead - 2 : lead - 2 + size]
        pool_four[0:lead] = jnp.zeros((lead, POOL_GROUP), jnp.float32)
        pool_four[lead:] = four
        eight = four + pool_four[lead - 4 : lead - 4 + size]
        sixteen = eight[tail:] + eight[tail - 8 : size - 8]
        sums = [two[tail:], four[tail:], eight[tail:], sixteen]
        picks = [c * pool_groups + group for c in range(cores)]
        running = chosen(core, [sums[pick] for pick in picks])
        reach = chosen(core, [jnp.float32(2 ** (pick + 1)) for pick in picks])
        share = 1.0 / jnp.minimum(position, reach)
        pooled = running * share - pool_in[0, :, cols].astype(jnp.float32)
        mixed = jnp.dot(
            pooled.astype(jnp.bfloat16),
            pool_weight[core * pool_groups + group],
            preferred_element_type=jnp.float32,
        )
        at = pl.multiple_of(core * pool + group * POOL_GROUP, POOL_GROUP)
        scale = pool_scale[:, pl.ds(at, POOL_GROUP)].astype(jnp.float32)
        out = inner + group * POOL_GROUP
        channels[:, out : out + POOL_GROUP] = (mixed * scale).astype(jnp.bfloat16)
        yield
    pool_letter().start()
    chain_point(1)
    for at in range(blocks):
        now = slice(at * BLOCK, (at + 1) * BLOCK)
        cum = cum_all[now, 0:heads]
        cum_flat = jnp.transpose(cum_all[now])
        step_flat = jnp.transpose(step_all[now])
        for group in range(groups):
            c_now = bc_conv[now, wide + group * STATE : wide + (group + 1) * STATE]
            scores = jnp.dot(
                c_now, b_turned[at * groups + group], preferred_element_type=jnp.float32
            )
            for pair in range(pairs):
                first = group * (span // HEAD_DIM) + 2 * pair
                both = []
                for head in (first, first + 1):
                    gap = cum[:, head : head + 1] - cum_flat[head : head + 1]
                    decay = jnp.exp(jnp.where(causal, gap, -1e30))
                    both.append((scores * decay * step_flat[head : head + 1]).astype(jnp.bfloat16))
                here = slice(first * HEAD_DIM, (first + 2) * HEAD_DIM)
                within[now, here] = jnp.dot(
                    jnp.concatenate(both, axis=1),
                    x_split[at, :, here],
                    preferred_element_type=jnp.float32,
                )
            yield
        if at == 0:
            chain_point(2)
    chain_point(3, True)
    yield
    falling = [None] * groups
    for at in range(blocks):
        now = slice(at * BLOCK, (at + 1) * BLOCK)
        for group in range(groups):
            cols = slice(group * span, (group + 1) * span)
            earlier = before[:, cols]
            if at:
                earlier = earlier * falling[group]
            entering = local_in[at, :, cols] + earlier
            c_now = bc_conv[now, wide + group * STATE : wide + (group + 1) * STATE]
            carried = jnp.dot(
                c_now, entering.astype(jnp.bfloat16), preferred_element_type=jnp.float32
            )
            mixed = (within[now, cols] + carried * grown[now, cols]) * silu(
                gate[0, now, cols].astype(jnp.float32)
            )
            root = lax.rsqrt(jnp.mean(mixed * mixed, axis=1, keepdims=True) + eps)
            at_gain = pl.multiple_of(core * inner + group * span, span)
            channels[now, cols] = (
                mixed * root * gain[:, pl.ds(at_gain, span)].astype(jnp.float32)
            ).astype(jnp.bfloat16)
            end = ends[at][group]
            falling[group] = end if at == 0 else falling[group] * end
        block_letter(at).start()
        yield
    letters = [pool_letter(), *(block_letter(at) for at in range(blocks))]

    def received():
        for letter in letters:
            letter.wait_recv()

    def finish():
        for letter in letters:
            letter.wait_send()

        @pl.when(follows)
        def _():
            for at in range(4):
                tails(at).wait_send()
            for group in range(groups):
                chain(group).wait_send()

    return received, finish


def whole_kernel(sp_size, fs_size, cores, tail, *refs):
    inputs, ssd_weight, pool_rows, out_gain, out = refs[:15], refs[15], refs[16], refs[17], refs[18]
    (z_sends, z_arrivals, y_sends, y_arrivals, m_sends, m_arrivals, p_sends, p_arrivals, o_sends,
     o_arrivals, local_sems, whole, parts, part_in, returned, return_in, squares, squares_in,
     *rest) = refs[19:]
    channels, far_channels = rest[-2:]
    links = Links(sp_size, fs_size)
    width = ssd_weight.shape[1]
    inner = ssd_weight.shape[0]
    rows = channels.shape[0]
    half = sp_size // cores
    core = links.core
    own_at = pl.multiple_of((links.z * 2 + links.y) * width, width)
    loads = [
        pltpu.make_async_copy(
            source, whole.at[pl.ds(begin, source.shape[0]), pl.ds(own_at, width)], local_sems.at[at]
        )
        for at, (source, begin) in enumerate(((ssd_weight, 0), (pool_rows, inner)))
    ]
    for load in loads:
        load.start()
    links.barrier()
    weights = Weights(links, whole, width, (z_sends, z_arrivals), (y_sends, y_arrivals))
    work = mixers(links, tail, cores, (*inputs, *rest), (m_sends, m_arrivals))

    def moves():
        for load in loads:
            load.wait()
        weights.begin()
        yield
        yield
        yield
        weights.turn()
        for step in range(1, sp_size):
            if step == 1:
                for _ in range(PAUSE):
                    yield
            for chunk in range(CHUNKS):
                yield
                weights.hop(step, chunk)
            yield step

    flow = moves()
    mixed = None
    hops = 0
    while mixed is None:
        try:
            next(work)
        except StopIteration as ended:
            mixed = ended.value
        else:
            hops = next(flow, None) or hops
    received, finish_mixers = mixed

    def reach(step):
        nonlocal hops
        while hops < step:
            hops = next(flow) or hops

    def multiply(turn, far):
        z = links.nearest(turn)
        source = far_channels if far else channels

        @pl.loop(0, 2)
        def _(y):
            slab = z * 2 + y
            at = pl.multiple_of(slab * width, width)
            parts[far, slab] = jnp.dot(
                source[...], whole[:, pl.ds(at, width)], preferred_element_type=jnp.float32
            ).astype(jnp.bfloat16)

            @pl.when(z // half != core)
            def _():
                part_letter(z, y, far).start()

    def part_letter(z, y, far):
        slab = z * 2 + y
        return remote(
            parts.at[far, slab],
            part_in.at[far, lax.rem(z, half) * 2 + y],
            p_sends,
            p_arrivals,
            far * 2 * sp_size + slab,
            links.sibling,
        )

    def return_letter(slot):
        return remote(
            returned.at[slot], return_in.at[slot], o_sends, o_arrivals, slot, links.beside
        )

    def give_back(turn):
        z = links.nearest(turn)

        @pl.when(z // half == core)
        def _():
            @pl.loop(0, 2)
            def _(y):
                part_letter(z, y, 1).wait_recv()
                slot = lax.rem(z, half) * 2 + y
                returned[slot] = (
                    parts[1, z * 2 + y].astype(jnp.float32) + part_in[1, slot].astype(jnp.float32)
                ).astype(jnp.bfloat16)
                return_letter(slot).start()

    weights.settle(0)
    multiply(0, 0)
    reach(1)
    weights.settle(1)
    multiply(1, 0)
    for step in range(2, sp_size):
        if step == sp_size - 1:
            received()
            for turn in range(step):
                multiply(turn, 1)
                if turn:
                    give_back(turn - 1)
            give_back(step - 1)
        reach(step)
        weights.settle(step)
        if step == sp_size - 1:
            multiply(step, 1)
            multiply(step, 0)
            give_back(step)
        else:
            multiply(step, 0)
    own_half = core * half
    slots = 2 * half

    def lane_squares(values):
        values = values * values
        total = values[:, 0:128]
        for at in range(1, width // 128):
            total = total + values[:, at * 128 : (at + 1) * 128]
        return total

    def own_total(slot):
        return parts[0, own_half * 2 + slot].astype(jnp.float32) + part_in[0, slot].astype(
            jnp.float32
        )

    squares[...] = jnp.zeros_like(squares)

    @pl.loop(0, slots)
    def _(slot):
        part_letter(own_half + slot // 2, lax.rem(slot, 2), 0).wait_recv()
        squares[...] += lane_squares(own_total(slot))

    @pl.loop(0, slots)
    def _(slot):
        return_letter(slot).wait_recv()
        squares[...] += lane_squares(return_in[slot].astype(jnp.float32))

    exchange = remote(squares, squares_in, o_sends, o_arrivals, slots, links.sibling)
    exchange.start()
    exchange.wait_recv()
    row_squares = jnp.sum(squares[...] + squares_in[...], axis=1, keepdims=True)
    root = lax.rsqrt(row_squares / out_gain.shape[1] + eps)

    @pl.loop(0, slots)
    def _(slot):
        first = (slot // 2) * fs_size + 2 * lax.rem(slot, 2)
        for values, x in (
            (own_total(slot), links.x),
            (return_in[slot].astype(jnp.float32), 1 - links.x),
        ):
            at = pl.multiple_of((first + x) * width, width)
            at_gain = pl.multiple_of(core * out.shape[2] + at, width)
            out[0, :, pl.ds(at, width)] = (
                values * root * out_gain[:, pl.ds(at_gain, width)].astype(jnp.float32)
            ).astype(jnp.bfloat16)

    exchange.wait_send()
    weights.finish()
    finish_mixers()

    @pl.loop(0, 2 * half)
    def _(slot):
        return_letter(slot).wait_send()
        other = (1 - core) * half
        for far in range(2):
            part_letter(other + slot // 2, lax.rem(slot, 2), far).wait_send()


def mixed_and_projected(inputs, ssd_weight, pool_rows, out_gain, tail):
    sp_size, fs_size, cores = lax.axis_size("sp"), lax.axis_size("fs"), lax.axis_size("tp")
    width = ssd_weight.shape[1]
    x_in, b_in, pool_in = inputs[0], inputs[2], inputs[12]
    tok_rows, inner = x_in.shape[1:]
    wide, pool = b_in.shape[2], pool_in.shape[2]
    groups = wide // STATE
    span = inner // groups
    blocks = tok_rows // BLOCK
    half = sp_size // cores
    slots = 2 * half
    vmem = pl.BlockSpec(memory_space=pltpu.VMEM)
    hbm = pl.BlockSpec(memory_space=pl.ANY)
    dma = pltpu.SemaphoreType.DMA
    half_type, full_type = jnp.bfloat16, jnp.float32
    z_spots, y_spots = CHUNKS * (sp_size - 1) * 4, CHUNKS * (2 * sp_size - 1)
    letters = 5 + groups + blocks
    return pl.pallas_call(
        functools.partial(whole_kernel, sp_size, fs_size, cores, tail),
        out_shape=jax.ShapeDtypeStruct((1, tok_rows, out_gain.shape[1] // cores), half_type),
        in_specs=[vmem] * len(inputs) + [hbm, hbm, vmem],
        out_specs=vmem,
        scratch_shapes=[
            dma((z_spots,)),
            dma((z_spots,)),
            dma((y_spots,)),
            dma((y_spots,)),
            dma((letters,)),
            dma((letters,)),
            dma((4 * sp_size,)),
            dma((4 * sp_size,)),
            dma((slots + 1,)),
            dma((slots + 1,)),
            dma((2,)),
            pltpu.VMEM((inner + pool, width * 2 * sp_size), half_type),
            pltpu.VMEM((2, 2 * sp_size, tok_rows, width), half_type),
            pltpu.VMEM((2, slots, tok_rows, width), half_type),
            pltpu.VMEM((slots, tok_rows, width), half_type),
            pltpu.VMEM((slots, tok_rows, width), half_type),
            pltpu.VMEM((tok_rows, 128), full_type),
            pltpu.VMEM((tok_rows, 128), full_type),
            pltpu.VMEM((tail, inner), half_type),
            pltpu.VMEM((tail, wide), half_type),
            pltpu.VMEM((tail, wide), half_type),
            pltpu.VMEM((tail, pool), half_type),
            pltpu.VMEM((tail + tok_rows, inner), full_type),
            pltpu.VMEM((tail + tok_rows, 2 * wide), full_type),
            pltpu.VMEM((8 + tail + tok_rows, pool), full_type),
            pltpu.VMEM((8 + tail + tok_rows, POOL_GROUP), full_type),
            pltpu.VMEM((8 + tail + tok_rows, POOL_GROUP), full_type),
            pltpu.VMEM((blocks, 2 * BLOCK, inner), half_type),
            pltpu.VMEM((tok_rows, 2 * wide), half_type),
            pltpu.VMEM((blocks * groups, STATE, BLOCK), half_type),
            pltpu.VMEM((tok_rows, 128), full_type),
            pltpu.VMEM((tok_rows, 128), full_type),
            pltpu.VMEM((tok_rows, inner), full_type),
            pltpu.VMEM((tok_rows, inner), full_type),
            pltpu.VMEM((blocks, STATE, inner), full_type),
            pltpu.VMEM((STATE, inner), full_type),
            pltpu.VMEM((STATE, inner), full_type),
            pltpu.VMEM((groups, STATE, span), half_type),
            pltpu.VMEM((groups, STATE, span), half_type),
            pltpu.VMEM((tok_rows, inner + pool), half_type),
            pltpu.VMEM((tok_rows, inner + pool), half_type),
        ],
        compiler_params=pltpu.CompilerParams(
            collective_id=0, has_side_effects=True, vmem_limit_bytes=56 * 2**20
        ),
        name="paired_mixers",
    )(*inputs, ssd_weight, pool_rows, out_gain)


def causal_taps(input_rows, prior_rows, tap_weights, offset_bias):
    padded = jnp.concatenate([prior_rows, input_rows], axis=0).astype(jnp.float32)
    tok_rows = input_rows.shape[0]
    running = jnp.zeros(input_rows.shape, jnp.float32) + offset_bias
    for tap_index in range(tap_weights.shape[0]):
        running = (
            running
            + tap_weights[tap_index].astype(jnp.float32) * padded[tap_index : tap_index + tok_rows]
        )
    return jax.nn.silu(running).astype(jnp.bfloat16)


def pool_mix(input_rows, prior_rows, positions, group_ids, local_weight, local_scale):
    tail_rows = prior_rows.shape[0]
    tok_rows = input_rows.shape[0]
    padded = jnp.concatenate([prior_rows, input_rows], axis=0).astype(jnp.float32)
    window_reach = jnp.left_shift(jnp.int32(2), group_ids)
    running = jnp.zeros(input_rows.shape, jnp.float32)
    for offset_back in range(tail_rows + 1):
        start_row = tail_rows - offset_back
        running = running + padded[start_row : start_row + tok_rows] * (
            offset_back < window_reach
        ).astype(jnp.float32)
    window_count = jnp.minimum(positions[:, None] + 1.0, window_reach.astype(jnp.float32)[None, :])
    pooled = (running / window_count - input_rows.astype(jnp.float32)).astype(jnp.bfloat16)
    grouped = pooled.reshape(tok_rows, local_weight.shape[0], local_weight.shape[1])
    mixed = jnp.einsum("lgc,gcd->lgd", grouped, local_weight, preferred_element_type=jnp.float32)
    return (mixed.reshape(input_rows.shape) * local_scale.astype(jnp.float32)).astype(jnp.bfloat16)


def join_states(earlier, later_part):
    return (
        earlier[0] + later_part[0],
        earlier[1] * jnp.exp(later_part[0])[..., None, None] + later_part[1],
    )


def body(
    statespace_input,
    output_gate_input,
    state_input_projection,
    state_output_projection,
    step_size_input,
    added_log_decay,
    logarithm_rates,
    head_channel_taps,
    input_projection_taps,
    output_projection_taps,
    input_projection_bias,
    group_norm_gain,
    pooling_input,
    pooling_group_weight,
    pooling_channel_scale,
    statespace_output_weight,
    pooling_output_weight,
    output_norm_gain,
):
    core_count = lax.axis_size("tp")
    sp_size, fs_size = lax.axis_size("sp"), lax.axis_size("fs")
    pool_tail = 2**POOL_GROUPS - 1
    paired = (
        statespace_output_weight.shape[1] % 128 == 0
        and fs_size == 4
        and core_count == 2
        and sp_size in (4, 8)
    )
    if paired:
        return mixed_and_projected(
            (
                statespace_input,
                output_gate_input,
                state_input_projection,
                state_output_projection,
                step_size_input,
                added_log_decay,
                logarithm_rates[None],
                head_channel_taps,
                input_projection_taps,
                output_projection_taps,
                input_projection_bias[None],
                group_norm_gain[None],
                pooling_input,
                pooling_group_weight,
                pooling_channel_scale[None],
            ),
            statespace_output_weight,
            pooling_output_weight,
            output_norm_gain[None],
            pool_tail + 1,
        )
    core_index = lax.axis_index("tp")
    seq_index = lax.axis_index("sp")
    head_channel_rows = statespace_input[0]
    output_gate_rows = output_gate_input[0]
    input_projection_rows = state_input_projection[0]
    output_projection_rows = state_output_projection[0]
    step_size_rows = step_size_input[0]
    decay_spikes = added_log_decay[0]
    pooling_rows = pooling_input[0]
    tok_rows = head_channel_rows.shape[0]
    inner_local = head_channel_rows.shape[1]
    heads_local = step_size_rows.shape[1]
    state_local = input_projection_rows.shape[1]
    pool_local = pooling_rows.shape[1]
    groups_local = state_local // STATE
    per_group = heads_local // groups_local
    groups_pool = pool_local // POOL_GROUP
    conv_tail = CONV - 1
    own_columns = jnp.concatenate([statespace_output_weight, pooling_output_weight], axis=0)
    tails = jnp.concatenate(
        [
            jnp.pad(rows[tok_rows - tail :], ((pool_tail - tail, 0), (0, 0)))
            for rows, tail in (
                (head_channel_rows, conv_tail),
                (input_projection_rows, conv_tail),
                (output_projection_rows, conv_tail),
                (pooling_rows, pool_tail),
            )
        ],
        axis=1,
    )
    prior = passed_along(tails, "sp", 1)
    widths = (inner_local, state_local, state_local, pool_local)
    prior_x, prior_b, prior_c, prior_pool = (
        prior[pool_tail - tail :, sum(widths[:at]) : sum(widths[: at + 1])]
        for at, tail in enumerate((conv_tail, conv_tail, conv_tail, pool_tail))
    )
    taps_x = lax.dynamic_slice_in_dim(head_channel_taps, core_index * inner_local, inner_local, 1)
    taps_b = lax.dynamic_slice_in_dim(
        input_projection_taps, core_index * state_local, state_local, 1
    )
    taps_c = lax.dynamic_slice_in_dim(
        output_projection_taps, core_index * state_local, state_local, 1
    )
    bias_b = lax.dynamic_slice_in_dim(
        input_projection_bias, core_index * state_local, state_local, 0
    )
    gain_ssd = lax.dynamic_slice_in_dim(group_norm_gain, core_index * inner_local, inner_local, 0)
    head_decay_rates = jnp.exp(
        lax.dynamic_slice_in_dim(logarithm_rates, core_index * heads_local, heads_local, 0)
    )
    gain_pool = lax.dynamic_slice_in_dim(
        pooling_channel_scale, core_index * pool_local, pool_local, 0
    )
    weight_pool = lax.dynamic_slice_in_dim(
        pooling_group_weight, core_index * groups_pool, groups_pool, 0
    )
    whole_columns = lax.all_gather(own_columns, ("sp", "fs"), axis=1, tiled=True)
    x_conv = causal_taps(head_channel_rows, prior_x, taps_x, 0.0)
    b_conv = causal_taps(input_projection_rows, prior_b, taps_b, bias_b.astype(jnp.float32))
    c_conv = causal_taps(output_projection_rows, prior_c, taps_c, 0.0)
    blocks = tok_rows // BLOCK
    discrete_step_size = jax.nn.softplus(step_size_rows.astype(jnp.float32))
    logarithm_decay = -discrete_step_size * head_decay_rates + decay_spikes
    cumulative_decay = jnp.cumsum(
        logarithm_decay.reshape(blocks, BLOCK, groups_local, per_group), axis=1
    )
    cum_t = cumulative_decay.transpose(0, 2, 3, 1)
    step_t = discrete_step_size.reshape(blocks, BLOCK, groups_local, per_group).transpose(
        0, 2, 3, 1
    )
    heads_x = x_conv.reshape(blocks, BLOCK, groups_local, per_group, HEAD_DIM)
    group_b = b_conv.reshape(blocks, BLOCK, groups_local, STATE)
    group_c = c_conv.reshape(blocks, BLOCK, groups_local, STATE)
    scores = jnp.einsum("ktgn,kugn->kgtu", group_c, group_b, preferred_element_type=jnp.float32)
    causal = jnp.arange(BLOCK)[:, None] >= jnp.arange(BLOCK)[None, :]
    decay_gap = cum_t[..., :, None] - cum_t[..., None, :]
    decay_factor = jnp.where(causal, jnp.exp(jnp.where(causal, decay_gap, 0.0)), 0.0)
    weights = (scores[:, :, None] * decay_factor * step_t[..., None, :]).astype(jnp.bfloat16)
    within = jnp.einsum("kgetu,kugep->ktgep", weights, heads_x, preferred_element_type=jnp.float32)
    block_end = cum_t[..., -1]
    end_weight = jnp.exp(block_end[..., None] - cum_t) * step_t
    scaled_x = (heads_x * end_weight.transpose(0, 3, 1, 2)[..., None]).astype(jnp.bfloat16)
    block_state = jnp.einsum(
        "kugep,kugn->kgepn", scaled_x, group_b, preferred_element_type=jnp.float32
    )

    def local_chain(state_now, current_inputs):
        piece_state, piece_fall = current_inputs
        return (state_now * jnp.exp(piece_fall)[..., None, None] + piece_state, state_now)

    final_state, local_entering = lax.scan(
        local_chain, jnp.zeros(block_state.shape[1:], jnp.float32), (block_state, block_end)
    )
    log_total = jnp.sum(block_end, axis=0)
    prefix_log = jnp.cumsum(block_end, axis=0) - block_end
    log_before, state_before = entering_2(
        (log_total, final_state),
        "sp",
        join_states,
        (jnp.zeros_like(log_total), jnp.zeros_like(final_state)),
    )
    entering = (local_entering + jnp.exp(prefix_log)[..., None, None] * state_before[None]).astype(
        jnp.bfloat16
    )
    carried_out = jnp.einsum(
        "ktgn,kgepn->ktgep", group_c, entering, preferred_element_type=jnp.float32
    )
    carried_out = carried_out * jnp.exp(cumulative_decay)[..., None]
    mixed_ssd = (within + carried_out).reshape(tok_rows, inner_local) * jax.nn.silu(
        output_gate_rows.astype(jnp.float32)
    )
    grouped = mixed_ssd.reshape(tok_rows, groups_local, inner_local // groups_local)
    normed = grouped * lax.rsqrt(jnp.mean(grouped * grouped, axis=-1, keepdims=True) + eps)
    ssd_out = (normed.reshape(tok_rows, inner_local) * gain_ssd.astype(jnp.float32)).astype(
        jnp.bfloat16
    )
    positions = (seq_index * tok_rows + jnp.arange(tok_rows, dtype=jnp.int32)).astype(jnp.float32)
    group_ids = core_index * groups_pool + jnp.arange(pool_local, dtype=jnp.int32) // POOL_GROUP
    pool_out = pool_mix(pooling_rows, prior_pool, positions, group_ids, weight_pool, gain_pool)
    channels = jnp.concatenate([ssd_out, pool_out], axis=1)
    half_width = D // core_count
    gain_out = lax.dynamic_slice_in_dim(
        output_norm_gain, core_index * half_width, half_width, 0
    ).astype(jnp.float32)
    partial = jnp.dot(channels, whole_columns, preferred_element_type=jnp.float32).astype(
        jnp.bfloat16
    )
    own_half = lax.dynamic_slice_in_dim(partial, core_index * half_width, half_width, 1).astype(
        jnp.float32
    )
    for hop in range(1, core_count):
        target = lax.rem(core_index + hop, core_count)
        leaving = lax.dynamic_slice_in_dim(partial, target * half_width, half_width, 1)
        route = [(i, (i + hop) % core_count) for i in range(core_count)]
        own_half = own_half + lax.ppermute(leaving, "tp", route).astype(jnp.float32)
    row_squares = lax.psum(jnp.sum(own_half * own_half, axis=1), "tp")
    result = own_half * lax.rsqrt(row_squares / D + eps)[:, None] * gain_out
    return result.astype(jnp.bfloat16)[None]


def solution(mesh):
    in_specs = (
        P("fs", "sp", "tp"),
        P("fs", "sp", "tp"),
        P("fs", "sp", "tp"),
        P("fs", "sp", "tp"),
        P("fs", "sp", "tp"),
        P("fs", "sp", "tp"),
        P(),
        P(),
        P(),
        P(),
        P(),
        P(),
        P("fs", "sp", "tp"),
        P(),
        P(),
        P("tp", ("sp", "fs")),
        P("tp", ("sp", "fs")),
        P(),
    )
    out_specs = P("fs", "sp", "tp")
    return jax.shard_map(body, mesh=mesh, in_specs=in_specs, out_specs=out_specs, check_vma=False)
```

time: 158 us -> 113 us (0.72)
  Pallas kernels: 117 us -> 101 us
  matrix products: 9.84 us -> 0 us
  other arithmetic: 8.26 us -> 0 us
  starting transfers between devices: 3.33 us -> 0 us
  waiting for transfers between devices: 3.24 us -> 0 us
  local copies, waits for them, and re-layouts: 13.4 us -> 10.8 us
  blocking collectives: 2.49 us -> 0 us
    pallas_call x1, Pallas kernels: 117 us -> 101 us  [mixed_and_projected(): pl.pallas_call(functools.partial(whole_kernel, sp_size, fs_size, cores, t...]
    dot_general x1 -> x0, matrix products: 9.84 us -> none  [body(): jnp.dot(channels, whole_columns, preferred_element_type=jnp.float32)]
    dynamic_slice x7 -> x0, local copies, waits for them, and re-layouts: 4.95 us -> none  [the longest x1 1.32 us: body(): lax.dynamic_slice_in_dim(partial, target * half_width, half_width, 1)]
    broadcast_in_dim x5 -> x4, local copies, waits for them, and re-layouts: 0.84 us -> 5.12 us  [the longest x1 1.31 us: body(): output_norm_gain[None]]
    broadcast_in_dim x1 -> x0, other arithmetic: 3.36 us -> none  [body(): return result.astype(jnp.bfloat16)[None]]
    ppermute x2 -> x0, starting transfers between devices: 3.33 us -> none  [the longest x1 2.05 us: body(): own_half = own_half + lax.ppermute(leaving, 'tp', route).astype(jnp.float32)]
    ppermute x2 -> x0, waiting for transfers between devices: 3.24 us -> none  [the longest x1 3.24 us: body(): own_half = own_half + lax.ppermute(leaving, 'tp', route).astype(jnp.float32)]
    unnamed x16 -> x3, local copies, waits for them, and re-layouts: 2.79 us -> 5.71 us
  transfers between devices with their start and end apart: 2 -> 0, of which waited for: 1 -> 0; matrix products, arithmetic and copies ran while one was open for 5% -> 0% of each run, Pallas kernels for 0% -> 0%
where the time goes in v1:
time: 113 us; the launch traced here: 112 us
  Pallas kernels  101 us (89%)
  local copies, waits for them, and re-layouts  10.8 us (10%)
    pallas_call x1, Pallas kernels, mixed_and_projected(): pl.pallas_call(functools.partial(whole_kernel, sp_size, fs_size, cores, t...  101 us
    unnamed x3, local copies, waits for them, and re-layouts  5.71 us

profile of v1, /device:TPU:25, one launch (start us, length us, event | category | flops | bytes accessed | tf_op | source)
XLA Modules:
  0.0 112.3 jit_solution(3207745793128467274)
XLA Ops:
  0.0 1.3 %broadcast_in_dim.16.refs_10_ = bf16[1,512]{1,0:T(2,128)(2,1)} reshape(bf16[512]{0:T(512)(128)(2,1)} %param.28) | data formatting | bytes 2048 | tf_op jit(solution)/shard_map/broadcast_in_dim | solution.py:810
  1.3 1.3 %broadcast_in_dim.18.refs_14_ = bf16[1,1024]{1,0:T(2,128)(2,1)} reshape(bf16[1024]{0:T(1024)(128)(2,1)} %param.32) | data formatting | bytes 4096 | tf_op jit(solution)/shard_map/broadcast_in_dim | solution.py:814
  2.5 1.3 %broadcast_in_dim.17.refs_11_ = bf16[1,2048]{1,0:T(2,128)(2,1)} reshape(bf16[2048]{0:T(1024)(128)(2,1)} %param.29) | data formatting | bytes 8192 | tf_op jit(solution)/shard_map/broadcast_in_dim | solution.py:811
  3.8 1.3 %broadcast_in_dim.19.refs_17_ = bf16[1,4096]{1,0:T(2,128)(2,1)} reshape(bf16[4096]{0:T(1024)(128)(2,1)} %param.35) | data formatting | bytes 16384 | tf_op jit(solution)/shard_map/broadcast_in_dim | solution.py:818
  5.1 1.4 %copy.19.refs_4_ = bf16[1,384,16]{2,1,0:T(8,128)(2,1)} copy(bf16[1,384,16]{1,2,0:T(8,128)(2,1)} %param.22) | data formatting | bytes 24576 | tf_op args[4]
  6.6 1.5 %copy.20.refs_5_ = f32[1,384,16]{2,1,0:T(8,128)} copy(f32[1,384,16]{1,2,0:T(8,128)} %param.23) | data formatting | bytes 49152 | tf_op args[5]
  8.1 101.5 %paired_mixers.1 = bf16[1,384,2048]{2,1,0:T(8,128)(2,1)} custom-call(bf16[1,384,1024]{2,1,0:T(8,128)(2,1)} %refs_0_.1, bf16[1,384,1024]{2,1,0:T(8,128)(2,1)} %refs_1_.1, bf16[1,384,256]{2,1,0:T(8,128)(2,1)} %refs_2_.1, bf16[1,384,256]{2,1,0:T(8,128)(2,1)} %refs_3_.1, bf16[1,384,16]{2,1,0:T(8,128)(2,1)} %copy.19.refs_4_, f32[1,384,16]{2,1,0:T(8,128)} %copy.20.refs_5_, ...), custom_call_target="tpu_custom_call" | custom-call | tf_op jit(solution)/shard_map/paired_mixers/pallas_call | solution.py:676
  109.6 2.7 %copy.22 = bf16[1,384,2048]{2,1,0:T(8,128)(2,1)} copy(bf16[1,384,2048]{2,1,0:T(8,128)(2,1)} %paired_mixers.1) | data formatting | bytes 3145728

commit v2 on v1

--- a/solution.py
+++ b/solution.py
@@ -48,7 +48,9 @@
 MESH_IDS = pl.DeviceIdType.MESH
 EXACT = lax.Precision.HIGHEST
 CHUNKS = 6
-PAUSE = 0
+INPUTS, GATE, VECTORS = 13, 1, 10
+SOURCES, OTHERS = (0, 2, 3, 11), (4, 5, 6, 7, 8, 9, 10, 12)
+ORDER = (*SOURCES, *OTHERS, GATE)
 
 
 class Links:
@@ -102,7 +104,7 @@
         self.rows = whole.shape[0] // CHUNKS
         self.direct = range(CHUNKS - 1)
         self.turned = (CHUNKS - 1,)
-        self.sent = []
+        self.sent = {}
 
     def region(self, chunk, z, y):
         at = pl.multiple_of((z * 2 + y) * self.width, self.width)
@@ -129,7 +131,7 @@
 
     def go(self, kind, *key):
         copy, here = kind(*key, False)
-        self.sent.append((kind, key))
+        self.sent[kind.__name__, key] = kind
         pl.when(here)(copy.start)
 
     def take(self, kind, *key):
@@ -141,32 +143,28 @@
             self.go(self.along, chunk, step, way, side)
 
     def begin(self):
-        for chunk in self.turned:
+        for chunk in (*self.turned, *self.direct):
             self.go(self.over, chunk, 0)
-        for chunk in self.direct:
+
+    def own(self, chunks, side=0):
+        for chunk in chunks:
             for way in (1, -1):
-                self.pass_on(chunk, 1, way, 0)
-            self.go(self.over, chunk, 0)
-        for chunk in self.turned:
-            for way in (1, -1):
-                self.pass_on(chunk, 1, way, 0)
+                self.pass_on(chunk, 1, way, side)
 
     def turn(self):
         for chunk in self.turned:
             self.take(self.over, chunk, 0)
+        for side in (0, 1):
+            self.own(self.turned, side)
+
+    def hop(self, step, chunks):
+        for chunk in chunks:
             for way in (1, -1):
-                self.pass_on(chunk, 1, way, 1)
-
-    def hop(self, step, chunk):
-        for way in (1, -1):
-            if chunk in self.turned:
-                for side in (0, 1):
+                for side in (0, 1) if chunk in self.turned else (0,):
                     self.take(self.along, chunk, step, way, side)
                     self.pass_on(chunk, step + 1, way, side)
-            else:
-                self.take(self.along, chunk, step, way, 0)
-                self.pass_on(chunk, step + 1, way, 0)
-                self.go(self.over, chunk, -way * step)
+                if chunk in self.direct:
+                    self.go(self.over, chunk, -way * step)
 
     def settle(self, step):
         for chunk in self.direct:
@@ -174,7 +172,7 @@
                 self.take(self.over, chunk, offset)
 
     def finish(self):
-        for kind, key in self.sent:
+        for (_, key), kind in self.sent.items():
             copy, here = kind(*key, False)
             pl.when(here)(copy.wait_send)
 
@@ -194,14 +192,14 @@
     return best
 
 
-def mixers(links, tail, cores, refs, sems):
-    (x_in, gate, b_in, c_in, dt, added, rates, x_taps, b_taps, c_taps, bias, gain, pool_in,
-     pool_weight, pool_scale, prior_x, prior_b, prior_c, prior_pool, x_pad, bc_pad, pool_pad,
-     pool_two, pool_four, x_split, bc_conv, b_turned, cum_all, step_all, within, grown, local_in,
+def mixers(links, tail, cores, pieces, fetches, refs, sems):
+    (x_in, gate, b_in, c_in, dt, added, rates, x_taps, b_taps, c_taps, vectors, pool_in,
+     pool_weight, prior_x, prior_b, prior_c, prior_pool, x_pad, bc_pad, pool_pad,
+     pool_two, pool_four, x_split, bc_conv, b_turned, flat, upright, within, grown, local_in,
      state, before, carry_in, carry_out, channels, far_channels) = refs
     sends, arrivals = sems
     rows, inner = x_in.shape[1:]
-    heads = dt.shape[2]
+    heads = dt.shape[1]
     wide = b_in.shape[2]
     pool = pool_in.shape[2]
     groups = wide // STATE
@@ -235,28 +233,30 @@
         )
 
     follows = z + 1 < links.n
+    for at in SOURCES:
+        fetches[at].wait()
 
     @pl.when(follows)
     def _():
         for at in range(4):
             tails(at).start()
 
-    yield
+    yield "start"
+    for at in OTHERS:
+        fetches[at].wait()
     x_pad[tail:] = x_in[0].astype(jnp.float32)
     bc_pad[tail:, 0:wide] = b_in[0].astype(jnp.float32)
     bc_pad[tail:, wide:] = c_in[0].astype(jnp.float32)
     pool_pad[0:lead] = jnp.zeros((lead, pool), jnp.float32)
     pool_pad[lead + tail :] = pool_in[0].astype(jnp.float32)
-    cum_all[...] = jnp.zeros_like(cum_all)
-    step_all[...] = jnp.zeros_like(step_all)
-    steps = softplus(dt[0].astype(jnp.float32))
-    step_all[:, 0:heads] = steps
-    own_rates = chosen(core, [rates[:, c * heads : (c + 1) * heads] for c in range(cores)])
-    logs = -steps * jnp.exp(own_rates) + added[0]
+    steps_flat = softplus(dt[0].astype(jnp.float32))
+    own_rates = rates[pl.ds(pl.multiple_of(core * heads, heads), heads)]
+    logs_flat = -steps_flat * jnp.exp(own_rates) + added[0]
+    flat[...] = jnp.zeros_like(flat)
     down = lax.broadcasted_iota(jnp.int32, (BLOCK, BLOCK), 0)
     over = lax.broadcasted_iota(jnp.int32, (BLOCK, BLOCK), 1)
     causal = down >= over
-    lower = causal.astype(jnp.float32)
+    upper = (down <= over).astype(jnp.float32)
     first_half = lax.broadcasted_iota(jnp.int32, (BLOCK, 2 * HEAD_DIM), 1) < HEAD_DIM
 
     def mine(ref, size):
@@ -265,7 +265,7 @@
 
     taps_x = mine(x_taps, inner)
     taps_bc = jnp.concatenate([mine(b_taps, wide), mine(c_taps, wide)], axis=1)
-    bias_b = mine(bias, wide)
+    bias_b = pieces(vectors, "bias", core * wide, wide)
     bias_bc = jnp.concatenate([bias_b, jnp.zeros_like(bias_b)], axis=1)
 
     @pl.when(z == 0)
@@ -299,7 +299,35 @@
             jnp.broadcast_to(narrow[:, head + 1 : head + 2], shape),
         )
 
-    yield
+    place = z * rows
+    position = (place + lax.broadcasted_iota(jnp.int32, (rows, 1), 0)).astype(jnp.float32) + 1.0
+    pool_groups = pool // POOL_GROUP
+    for group in range(pool_groups):
+        cols = slice(group * POOL_GROUP, (group + 1) * POOL_GROUP)
+        size = rows + tail
+        two = pool_pad[lead:, cols] + pool_pad[lead - 1 : lead - 1 + size, cols]
+        pool_two[0:lead] = jnp.zeros((lead, POOL_GROUP), jnp.float32)
+        pool_two[lead:] = two
+        four = two + pool_two[lead - 2 : lead - 2 + size]
+        pool_four[0:lead] = jnp.zeros((lead, POOL_GROUP), jnp.float32)
+        pool_four[lead:] = four
+        eight = four + pool_four[lead - 4 : lead - 4 + size]
+        sixteen = eight[tail:] + eight[tail - 8 : size - 8]
+        sums = [two[tail:], four[tail:], eight[tail:], sixteen]
+        picks = [c * pool_groups + group for c in range(cores)]
+        running = chosen(core, [sums[pick] for pick in picks])
+        reach = chosen(core, [jnp.float32(2 ** (pick + 1)) for pick in picks])
+        share = 1.0 / jnp.minimum(position, reach)
+        pooled = running * share - pool_in[0, :, cols].astype(jnp.float32)
+        mixed = jnp.dot(
+            pooled.astype(jnp.bfloat16),
+            pool_weight[core * pool_groups + group],
+            preferred_element_type=jnp.float32,
+        )
+        scale = pieces(vectors, "scale", core * pool + group * POOL_GROUP, POOL_GROUP)
+        out = inner + group * POOL_GROUP
+        channels[:, out : out + POOL_GROUP] = (mixed * scale).astype(jnp.bfloat16)
+    pool_letter().start()
     pairs = span // (2 * HEAD_DIM)
     ends = []
     state[...] = jnp.zeros_like(state)
@@ -308,10 +336,14 @@
         bc_conv[now] = silu(taps(bc_pad, taps_bc, at, slice(0, 2 * wide)) + bias_bc).astype(
             jnp.bfloat16
         )
-        cum = jnp.dot(lower, logs[now], precision=EXACT, preferred_element_type=jnp.float32)
-        cum_all[now, 0:heads] = cum
+        flat[at, 0:heads] = jnp.dot(
+            logs_flat[:, now], upper, precision=EXACT, preferred_element_type=jnp.float32
+        )
+        flat[at, heads : 2 * heads] = steps_flat[:, now]
+        upright[at] = jnp.transpose(flat[at])
+        cum = upright[at, :, 0:heads]
         decayed = jnp.exp(cum)
-        closing = jnp.exp(cum[BLOCK - 1 : BLOCK] - cum) * steps[now]
+        closing = jnp.exp(cum[BLOCK - 1 : BLOCK] - cum) * upright[at, :, heads : 2 * heads]
         ended = []
         for group in range(groups):
             cols = slice(group * span, (group + 1) * span)
@@ -338,7 +370,7 @@
             state[:, cols] = state[:, cols] * end + jnp.dot(
                 b_flat, jnp.concatenate(scaled, axis=1), preferred_element_type=jnp.float32
             )
-            yield
+        yield at
         ends.append(ended)
 
     def hand_on():
@@ -366,44 +398,12 @@
         pl.when(z >= place if last else z == place)(hand_on)
 
     chain_point(0)
-    yield
-    place = z * rows
-    position = (place + lax.broadcasted_iota(jnp.int32, (rows, 1), 0)).astype(jnp.float32) + 1.0
-    pool_groups = pool // POOL_GROUP
-    for group in range(pool_groups):
-        cols = slice(group * POOL_GROUP, (group + 1) * POOL_GROUP)
-        size = rows + tail
-        two = pool_pad[lead:, cols] + pool_pad[lead - 1 : lead - 1 + size, cols]
-        pool_two[0:lead] = jnp.zeros((lead, POOL_GROUP), jnp.float32)
-        pool_two[lead:] = two
-        four = two + pool_two[lead - 2 : lead - 2 + size]
-        pool_four[0:lead] = jnp.zeros((lead, POOL_GROUP), jnp.float32)
-        pool_four[lead:] = four
-        eight = four + pool_four[lead - 4 : lead - 4 + size]
-        sixteen = eight[tail:] + eight[tail - 8 : size - 8]
-        sums = [two[tail:], four[tail:], eight[tail:], sixteen]
-        picks = [c * pool_groups + group for c in range(cores)]
-        running = chosen(core, [sums[pick] for pick in picks])
-        reach = chosen(core, [jnp.float32(2 ** (pick + 1)) for pick in picks])
-        share = 1.0 / jnp.minimum(position, reach)
-        pooled = running * share - pool_in[0, :, cols].astype(jnp.float32)
-        mixed = jnp.dot(
-            pooled.astype(jnp.bfloat16),
-            pool_weight[core * pool_groups + group],
-            preferred_element_type=jnp.float32,
-        )
-        at = pl.multiple_of(core * pool + group * POOL_GROUP, POOL_GROUP)
-        scale = pool_scale[:, pl.ds(at, POOL_GROUP)].astype(jnp.float32)
-        out = inner + group * POOL_GROUP
-        channels[:, out : out + POOL_GROUP] = (mixed * scale).astype(jnp.bfloat16)
-        yield
-    pool_letter().start()
-    chain_point(1)
+    yield "states"
     for at in range(blocks):
         now = slice(at * BLOCK, (at + 1) * BLOCK)
-        cum = cum_all[now, 0:heads]
-        cum_flat = jnp.transpose(cum_all[now])
-        step_flat = jnp.transpose(step_all[now])
+        cum = upright[at, :, 0:heads]
+        cum_flat = flat[at, 0:heads]
+        step_flat = flat[at, heads : 2 * heads]
         for group in range(groups):
             c_now = bc_conv[now, wide + group * STATE : wide + (group + 1) * STATE]
             scores = jnp.dot(
@@ -422,12 +422,13 @@
                     x_split[at, :, here],
                     preferred_element_type=jnp.float32,
                 )
-            yield
-        if at == 0:
-            chain_point(2)
+    chain_point(1)
+    yield "second"
+    chain_point(2)
+    yield "third"
     chain_point(3, True)
-    yield
     falling = [None] * groups
+    fetches[GATE].wait()
     for at in range(blocks):
         now = slice(at * BLOCK, (at + 1) * BLOCK)
         for group in range(groups):
@@ -444,14 +445,11 @@
                 gate[0, now, cols].astype(jnp.float32)
             )
             root = lax.rsqrt(jnp.mean(mixed * mixed, axis=1, keepdims=True) + eps)
-            at_gain = pl.multiple_of(core * inner + group * span, span)
-            channels[now, cols] = (
-                mixed * root * gain[:, pl.ds(at_gain, span)].astype(jnp.float32)
-            ).astype(jnp.bfloat16)
+            gain = pieces(vectors, "gain", core * inner + group * span, span)
+            channels[now, cols] = (mixed * root * gain).astype(jnp.bfloat16)
             end = ends[at][group]
             falling[group] = end if at == 0 else falling[group] * end
         block_letter(at).start()
-        yield
     letters = [pool_letter(), *(block_letter(at) for at in range(blocks))]
 
     def received():
@@ -472,11 +470,13 @@
     return received, finish
 
 
-def whole_kernel(sp_size, fs_size, cores, tail, *refs):
-    inputs, ssd_weight, pool_rows, out_gain, out = refs[:15], refs[15], refs[16], refs[17], refs[18]
+def whole_kernel(sp_size, fs_size, cores, tail, pieces, *refs):
+    inputs, ssd_weight, pool_rows, out = refs[:INPUTS], *refs[INPUTS : INPUTS + 3]
     (z_sends, z_arrivals, y_sends, y_arrivals, m_sends, m_arrivals, p_sends, p_arrivals, o_sends,
      o_arrivals, local_sems, whole, parts, part_in, returned, return_in, squares, squares_in,
-     *rest) = refs[19:]
+     *rest) = refs[INPUTS + 3 :]
+    held, rest = rest[:INPUTS], rest[INPUTS:]
+    vectors = held[VECTORS]
     channels, far_channels = rest[-2:]
     links = Links(sp_size, fs_size)
     width = ssd_weight.shape[1]
@@ -491,45 +491,43 @@
         )
         for at, (source, begin) in enumerate(((ssd_weight, 0), (pool_rows, inner)))
     ]
+    fetches = [
+        pltpu.make_async_copy(source, place, local_sems.at[2 + at])
+        for at, (source, place) in enumerate(zip(inputs, held))
+    ]
+    for at in ORDER:
+        fetches[at].start()
     for load in loads:
         load.start()
     links.barrier()
     weights = Weights(links, whole, width, (z_sends, z_arrivals), (y_sends, y_arrivals))
-    work = mixers(links, tail, cores, (*inputs, *rest), (m_sends, m_arrivals))
-
-    def moves():
-        for load in loads:
-            load.wait()
-        weights.begin()
-        yield
-        yield
-        yield
-        weights.turn()
-        for step in range(1, sp_size):
-            if step == 1:
-                for _ in range(PAUSE):
-                    yield
-            for chunk in range(CHUNKS):
-                yield
-                weights.hop(step, chunk)
-            yield step
-
-    flow = moves()
+    work = mixers(links, tail, cores, pieces, fetches, (*held, *rest), (m_sends, m_arrivals))
+
+    direct, turned = weights.direct, weights.turned
+    late = links.z >= sp_size // 2
     mixed = None
-    hops = 0
     while mixed is None:
         try:
-            next(work)
+            mark = next(work)
         except StopIteration as ended:
             mixed = ended.value
-        else:
-            hops = next(flow, None) or hops
+            break
+        if mark == "start":
+            for load in loads:
+                load.wait()
+            weights.begin()
+            weights.own(direct[:3])
+        elif mark == 1:
+            weights.own(direct[3:4])
+        elif mark == "states":
+            weights.own(direct[4:])
+            weights.hop(1, direct[:1])
+        elif mark == "second":
+            pl.when(late)(lambda: weights.hop(1, direct[1:3]))
+        elif mark == "third":
+            pl.when(late)(lambda: weights.hop(1, direct[3:]))
     received, finish_mixers = mixed
-
-    def reach(step):
-        nonlocal hops
-        while hops < step:
-            hops = next(flow) or hops
+    pl.when(jnp.logical_not(late))(lambda: weights.hop(1, direct[1:]))
 
     def multiply(turn, far):
         z = links.nearest(turn)
@@ -577,27 +575,32 @@
                 ).astype(jnp.bfloat16)
                 return_letter(slot).start()
 
+    last = sp_size - 1
+    weights.turn()
     weights.settle(0)
     multiply(0, 0)
-    reach(1)
-    weights.settle(1)
-    multiply(1, 0)
     for step in range(2, sp_size):
-        if step == sp_size - 1:
-            received()
-            for turn in range(step):
-                multiply(turn, 1)
-                if turn:
-                    give_back(turn - 1)
-            give_back(step - 1)
-        reach(step)
-        weights.settle(step)
-        if step == sp_size - 1:
-            multiply(step, 1)
-            multiply(step, 0)
-            give_back(step)
-        else:
-            multiply(step, 0)
+        weights.hop(step, direct)
+        if step < last:
+            weights.hop(step - 1, turned)
+            weights.settle(step - 1)
+            multiply(step - 1, 0)
+    received()
+    for turn in range(last - 1):
+        multiply(turn, 1)
+        if turn:
+            give_back(turn - 1)
+    weights.hop(last - 1, turned)
+    weights.settle(last - 1)
+    multiply(last - 1, 1)
+    give_back(last - 2)
+    multiply(last - 1, 0)
+    give_back(last - 1)
+    weights.hop(last, turned)
+    weights.settle(last)
+    multiply(last, 1)
+    multiply(last, 0)
+    give_back(last)
     own_half = core * half
     slots = 2 * half
 
@@ -629,7 +632,8 @@
     exchange.start()
     exchange.wait_recv()
     row_squares = jnp.sum(squares[...] + squares_in[...], axis=1, keepdims=True)
-    root = lax.rsqrt(row_squares / out_gain.shape[1] + eps)
+    features = cores * out.shape[2]
+    root = lax.rsqrt(row_squares / features + eps)
 
     @pl.loop(0, slots)
     def _(slot):
@@ -639,10 +643,8 @@
             (return_in[slot].astype(jnp.float32), 1 - links.x),
         ):
             at = pl.multiple_of((first + x) * width, width)
-            at_gain = pl.multiple_of(core * out.shape[2] + at, width)
-            out[0, :, pl.ds(at, width)] = (
-                values * root * out_gain[:, pl.ds(at_gain, width)].astype(jnp.float32)
-            ).astype(jnp.bfloat16)
+            gain = pieces(vectors, "out", core * out.shape[2] + at, width)
+            out[0, :, pl.ds(at, width)] = (values * root * gain).astype(jnp.bfloat16)
 
     exchange.wait_send()
     weights.finish()
@@ -656,10 +658,20 @@
             part_letter(other + slot // 2, lax.rem(slot, 2), far).wait_send()
 
 
-def mixed_and_projected(inputs, ssd_weight, pool_rows, out_gain, tail):
+def mixed_and_projected(inputs, vectors, ssd_weight, pool_rows, tail):
     sp_size, fs_size, cores = lax.axis_size("sp"), lax.axis_size("fs"), lax.axis_size("tp")
     width = ssd_weight.shape[1]
-    x_in, b_in, pool_in = inputs[0], inputs[2], inputs[12]
+    x_in, b_in, pool_in = inputs[0], inputs[2], inputs[10]
+    starts, features = {}, vectors["out"].shape[0]
+    for name, vector in vectors.items():
+        starts[name] = sum(vectors[other].shape[0] for other in starts)
+
+    def pieces(ref, name, offset, size):
+        at = pl.multiple_of(starts[name] + offset, 128)
+        return ref[:, pl.ds(at, size)].astype(jnp.float32)
+
+    joined = jnp.concatenate(list(vectors.values()))[None]
+    inputs = (*inputs[:10], joined, *inputs[10:])
     tok_rows, inner = x_in.shape[1:]
     wide, pool = b_in.shape[2], pool_in.shape[2]
     groups = wide // STATE
@@ -668,15 +680,15 @@
     half = sp_size // cores
     slots = 2 * half
     vmem = pl.BlockSpec(memory_space=pltpu.VMEM)
-    hbm = pl.BlockSpec(memory_space=pl.ANY)
+    hbm = pl.BlockSpec(memory_space=pltpu.HBM)
     dma = pltpu.SemaphoreType.DMA
     half_type, full_type = jnp.bfloat16, jnp.float32
     z_spots, y_spots = CHUNKS * (sp_size - 1) * 4, CHUNKS * (2 * sp_size - 1)
     letters = 5 + groups + blocks
     return pl.pallas_call(
-        functools.partial(whole_kernel, sp_size, fs_size, cores, tail),
-        out_shape=jax.ShapeDtypeStruct((1, tok_rows, out_gain.shape[1] // cores), half_type),
-        in_specs=[vmem] * len(inputs) + [hbm, hbm, vmem],
+        functools.partial(whole_kernel, sp_size, fs_size, cores, tail, pieces),
+        out_shape=jax.ShapeDtypeStruct((1, tok_rows, features // cores), half_type),
+        in_specs=[hbm] * (len(inputs) + 2),
         out_specs=vmem,
         scratch_shapes=[
             dma((z_spots,)),
@@ -689,7 +701,7 @@
             dma((4 * sp_size,)),
             dma((slots + 1,)),
             dma((slots + 1,)),
-            dma((2,)),
+            dma((2 + len(inputs),)),
             pltpu.VMEM((inner + pool, width * 2 * sp_size), half_type),
             pltpu.VMEM((2, 2 * sp_size, tok_rows, width), half_type),
             pltpu.VMEM((2, slots, tok_rows, width), half_type),
@@ -697,6 +709,7 @@
             pltpu.VMEM((slots, tok_rows, width), half_type),
             pltpu.VMEM((tok_rows, 128), full_type),
             pltpu.VMEM((tok_rows, 128), full_type),
+            *(pltpu.VMEM(array.shape, array.dtype) for array in inputs),
             pltpu.VMEM((tail, inner), half_type),
             pltpu.VMEM((tail, wide), half_type),
             pltpu.VMEM((tail, wide), half_type),
@@ -709,8 +722,8 @@
             pltpu.VMEM((blocks, 2 * BLOCK, inner), half_type),
             pltpu.VMEM((tok_rows, 2 * wide), half_type),
             pltpu.VMEM((blocks * groups, STATE, BLOCK), half_type),
-            pltpu.VMEM((tok_rows, 128), full_type),
-            pltpu.VMEM((tok_rows, 128), full_type),
+            pltpu.VMEM((blocks, 128, BLOCK), full_type),
+            pltpu.VMEM((blocks, BLOCK, 128), full_type),
             pltpu.VMEM((tok_rows, inner), full_type),
             pltpu.VMEM((tok_rows, inner), full_type),
             pltpu.VMEM((blocks, STATE, inner), full_type),
@@ -722,10 +735,10 @@
             pltpu.VMEM((tok_rows, inner + pool), half_type),
         ],
         compiler_params=pltpu.CompilerParams(
-            collective_id=0, has_side_effects=True, vmem_limit_bytes=56 * 2**20
+            collective_id=0, has_side_effects=True, vmem_limit_bytes=54 * 2**20
         ),
         name="paired_mixers",
-    )(*inputs, ssd_weight, pool_rows, out_gain)
+    )(*inputs, ssd_weight, pool_rows)
 
 
 def causal_taps(input_rows, prior_rows, tap_weights, offset_bias):
@@ -801,21 +814,23 @@
                 output_gate_input,
                 state_input_projection,
                 state_output_projection,
-                step_size_input,
-                added_log_decay,
-                logarithm_rates[None],
+                jnp.swapaxes(step_size_input, 1, 2),
+                jnp.swapaxes(added_log_decay, 1, 2),
+                logarithm_rates[:, None],
                 head_channel_taps,
                 input_projection_taps,
                 output_projection_taps,
-                input_projection_bias[None],
-                group_norm_gain[None],
                 pooling_input,
                 pooling_group_weight,
-                pooling_channel_scale[None],
             ),
+            {
+                "out": output_norm_gain,
+                "gain": group_norm_gain,
+                "scale": pooling_channel_scale,
+                "bias": input_projection_bias,
+            },
             statespace_output_weight,
             pooling_output_weight,
-            output_norm_gain[None],
             pool_tail + 1,
         )
     core_index = lax.axis_index("tp")

time: 113 us -> 94 us (0.83)
  the two profiles are of different devices: /device:TPU:25 before, /device:TPU:0 now
where the time goes in v2:
time: 94 us; the launch traced here: 93.8 us
  Pallas kernels  88.4 us (94%)
  local copies, waits for them, and re-layouts  4.69 us (5%)
    pallas_call x1, Pallas kernels, mixed_and_projected(): pl.pallas_call(functools.partial(whole_kernel, sp_size, fs_size, cores, t...  88.4 us
    unnamed x1, local copies, waits for them, and re-layouts  2.73 us

profile of v2, /device:TPU:0, one launch (start us, length us, event | category | flops | bytes accessed | tf_op | source)
XLA Modules:
  0.0 93.8 jit_solution(13021284566243422344)
XLA Ops:
  0.0 1.3 %copy.19.refs_6_ = f32[32,1]{1,0:T(8,128)} copy(f32[32,1]{0,1:T(1,128)} %bitcast.5) | data formatting | bytes 256 | tf_op jit(solution)/shard_map/broadcast_in_dim | solution.py:819
  1.3 0.8 pad_maximum_fusion
  2.1 0.6 broadcast_in_dim.7.refs_10_
  2.7 88.4 %paired_mixers.1 = bf16[1,384,2048]{2,1,0:T(8,128)(2,1)} custom-call(bf16[1,384,1024]{2,1,0:T(8,128)(2,1)} %refs_0_.1, bf16[1,384,1024]{2,1,0:T(8,128)(2,1)} %refs_1_.1, bf16[1,384,256]{2,1,0:T(8,128)(2,1)} %refs_2_.1, bf16[1,384,256]{2,1,0:T(8,128)(2,1)} %refs_3_.1, bf16[1,16,384]{2,1,0:T(8,128)(2,1)} %bitcast.4, f32[1,16,384]{2,1,0:T(8,128)} %bitcast.3, ...), custom_call_target="tpu_custom_call" | custom-call | tf_op jit(solution)/shard_map/paired_mixers/pallas_call | solution.py:688
  91.1 2.7 %copy.21 = bf16[1,384,2048]{2,1,0:T(8,128)(2,1)} copy(bf16[1,384,2048]{2,1,0:T(8,128)(2,1)} %paired_mixers.1) | data formatting | bytes 3145728

commit v3 on v2

--- a/solution.py
+++ b/solution.py
@@ -47,10 +47,9 @@
 
 MESH_IDS = pl.DeviceIdType.MESH
 EXACT = lax.Precision.HIGHEST
-CHUNKS = 6
+CHUNKS, CHAINS = 6, 4
 INPUTS, GATE, VECTORS = 13, 1, 10
 SOURCES, OTHERS = (0, 2, 3, 11), (4, 5, 6, 7, 8, 9, 10, 12)
-ORDER = (*SOURCES, *OTHERS, GATE)
 
 
 class Links:
@@ -139,37 +138,43 @@
         pl.when(here)(copy.wait_recv)
 
     def pass_on(self, chunk, step, way, side):
-        if step < self.links.n:
+        if step < self.links.n and not self.single(step, way, side):
             self.go(self.along, chunk, step, way, side)
+
+    def single(self, step, way, side):
+        return step >= self.links.n - 2 and way == 1 and side == 1
 
     def begin(self):
         for chunk in (*self.turned, *self.direct):
             self.go(self.over, chunk, 0)
 
-    def own(self, chunks, side=0):
+    def own(self, chunks, sides=(0,), ways=(1, -1)):
         for chunk in chunks:
-            for way in (1, -1):
-                self.pass_on(chunk, 1, way, side)
+            for side in sides:
+                for way in ways:
+                    self.pass_on(chunk, 1, way, side)
 
     def turn(self):
         for chunk in self.turned:
             self.take(self.over, chunk, 0)
-        for side in (0, 1):
-            self.own(self.turned, side)
-
-    def hop(self, step, chunks):
+
+    def hop(self, step, chunks, sides=(0,), ways=(1, -1)):
         for chunk in chunks:
-            for way in (1, -1):
-                for side in (0, 1) if chunk in self.turned else (0,):
-                    self.take(self.along, chunk, step, way, side)
-                    self.pass_on(chunk, step + 1, way, side)
-                if chunk in self.direct:
+            for way in ways:
+                for side in sides:
+                    if not self.single(step, way, side):
+                        self.take(self.along, chunk, step, way, side)
+                        self.pass_on(chunk, step + 1, way, side)
+                if chunk in self.direct or (0 in sides and self.single(step, way, 1)):
                     self.go(self.over, chunk, -way * step)
 
     def settle(self, step):
         for chunk in self.direct:
             for offset in (0,) if step == 0 else (step, -step):
                 self.take(self.over, chunk, offset)
+        if self.single(step, 1, 1):
+            for chunk in self.turned:
+                self.take(self.over, chunk, -step)
 
     def finish(self):
         for (_, key), kind in self.sent.items():
@@ -207,6 +212,8 @@
     blocks = rows // BLOCK
     z, core = links.z, links.core
     lead = 8
+    parts = CHAINS
+    length = inner // parts
     sources = ((x_in, prior_x), (b_in, prior_b), (c_in, prior_c), (pool_in, prior_pool))
 
     def tails(at):
@@ -223,13 +230,13 @@
     def pool_letter():
         cols = pl.ds(inner, pool)
         return remote(
-            channels.at[:, cols], far_channels.at[:, cols], sends, arrivals, 4 + groups, links.beside
+            channels.at[:, cols], far_channels.at[:, cols], sends, arrivals, 4 + parts, links.beside
         )
 
     def block_letter(at):
         place = (pl.ds(at * BLOCK, BLOCK), pl.ds(0, inner))
         return remote(
-            channels.at[place], far_channels.at[place], sends, arrivals, 5 + groups + at, links.beside
+            channels.at[place], far_channels.at[place], sends, arrivals, 5 + parts + at, links.beside
         )
 
     follows = z + 1 < links.n
@@ -250,7 +257,13 @@
     pool_pad[0:lead] = jnp.zeros((lead, pool), jnp.float32)
     pool_pad[lead + tail :] = pool_in[0].astype(jnp.float32)
     steps_flat = softplus(dt[0].astype(jnp.float32))
-    own_rates = rates[pl.ds(pl.multiple_of(core * heads, heads), heads)]
+    table = (heads, rates.shape[1])
+    picked = lax.broadcasted_iota(jnp.int32, table, 1) == (
+        core * heads + lax.broadcasted_iota(jnp.int32, table, 0)
+    )
+    own_rates = jnp.sum(
+        jnp.where(picked, jnp.broadcast_to(rates[...], table), 0.0), axis=1, keepdims=True
+    )
     logs_flat = -steps_flat * jnp.exp(own_rates) + added[0]
     flat[...] = jnp.zeros_like(flat)
     down = lax.broadcasted_iota(jnp.int32, (BLOCK, BLOCK), 0)
@@ -299,35 +312,6 @@
             jnp.broadcast_to(narrow[:, head + 1 : head + 2], shape),
         )
 
-    place = z * rows
-    position = (place + lax.broadcasted_iota(jnp.int32, (rows, 1), 0)).astype(jnp.float32) + 1.0
-    pool_groups = pool // POOL_GROUP
-    for group in range(pool_groups):
-        cols = slice(group * POOL_GROUP, (group + 1) * POOL_GROUP)
-        size = rows + tail
-        two = pool_pad[lead:, cols] + pool_pad[lead - 1 : lead - 1 + size, cols]
-        pool_two[0:lead] = jnp.zeros((lead, POOL_GROUP), jnp.float32)
-        pool_two[lead:] = two
-        four = two + pool_two[lead - 2 : lead - 2 + size]
-        pool_four[0:lead] = jnp.zeros((lead, POOL_GROUP), jnp.float32)
-        pool_four[lead:] = four
-        eight = four + pool_four[lead - 4 : lead - 4 + size]
-        sixteen = eight[tail:] + eight[tail - 8 : size - 8]
-        sums = [two[tail:], four[tail:], eight[tail:], sixteen]
-        picks = [c * pool_groups + group for c in range(cores)]
-        running = chosen(core, [sums[pick] for pick in picks])
-        reach = chosen(core, [jnp.float32(2 ** (pick + 1)) for pick in picks])
-        share = 1.0 / jnp.minimum(position, reach)
-        pooled = running * share - pool_in[0, :, cols].astype(jnp.float32)
-        mixed = jnp.dot(
-            pooled.astype(jnp.bfloat16),
-            pool_weight[core * pool_groups + group],
-            preferred_element_type=jnp.float32,
-        )
-        scale = pieces(vectors, "scale", core * pool + group * POOL_GROUP, POOL_GROUP)
-        out = inner + group * POOL_GROUP
-        channels[:, out : out + POOL_GROUP] = (mixed * scale).astype(jnp.bfloat16)
-    pool_letter().start()
     pairs = span // (2 * HEAD_DIM)
     ends = []
     state[...] = jnp.zeros_like(state)
@@ -378,27 +362,56 @@
         def _():
             before[...] = jnp.zeros_like(before)
 
-        for group in range(groups):
-            cols = slice(group * span, (group + 1) * span)
+        for link in range(parts):
+            cols = slice(link * length, (link + 1) * length)
+            group, at_end = link * length // span, slice(link * length % span, link * length % span + length)
 
             @pl.when(z > 0)
-            def _(group=group, cols=cols):
-                chain(group).wait_recv()
-                before[:, cols] = carry_in[group].astype(jnp.float32)
+            def _(link=link, cols=cols):
+                chain(link).wait_recv()
+                before[:, cols] = carry_in[link].astype(jnp.float32)
 
             @pl.when(follows)
-            def _(group=group, cols=cols):
-                falling = ends[0][group]
+            def _(link=link, cols=cols, group=group, at_end=at_end):
+                falling = ends[0][group][:, at_end]
                 for at in range(1, blocks):
-                    falling = falling * ends[at][group]
-                carry_out[group] = (before[:, cols] * falling + state[:, cols]).astype(jnp.bfloat16)
-                chain(group).start()
+                    falling = falling * ends[at][group][:, at_end]
+                carry_out[link] = (before[:, cols] * falling + state[:, cols]).astype(jnp.bfloat16)
+                chain(link).start()
 
     def chain_point(place, last=False):
         pl.when(z >= place if last else z == place)(hand_on)
 
     chain_point(0)
     yield "states"
+    place = z * rows
+    position = (place + lax.broadcasted_iota(jnp.int32, (rows, 1), 0)).astype(jnp.float32) + 1.0
+    pool_groups = pool // POOL_GROUP
+    for group in range(pool_groups):
+        cols = slice(group * POOL_GROUP, (group + 1) * POOL_GROUP)
+        size = rows + tail
+        two = pool_pad[lead:, cols] + pool_pad[lead - 1 : lead - 1 + size, cols]
+        pool_two[0:lead] = jnp.zeros((lead, POOL_GROUP), jnp.float32)
+        pool_two[lead:] = two
+        four = two + pool_two[lead - 2 : lead - 2 + size]
+        pool_four[0:lead] = jnp.zeros((lead, POOL_GROUP), jnp.float32)
+        pool_four[lead:] = four
+        eight = four + pool_four[lead - 4 : lead - 4 + size]
+        sixteen = eight[tail:] + eight[tail - 8 : size - 8]
+        sums = [two[tail:], four[tail:], eight[tail:], sixteen]
+        picks = [c * pool_groups + group for c in range(cores)]
+        running = chosen(core, [sums[pick] for pick in picks])
+        reach = chosen(core, [jnp.float32(2 ** (pick + 1)) for pick in picks])
+        pooled = running / jnp.minimum(position, reach) - pool_in[0, :, cols].astype(jnp.float32)
+        mixed = jnp.dot(
+            pooled.astype(jnp.bfloat16),
+            pool_weight[core * pool_groups + group],
+            preferred_element_type=jnp.float32,
+        )
+        scale = pieces(vectors, "scale", core * pool + group * POOL_GROUP, POOL_GROUP)
+        out = inner + group * POOL_GROUP
+        channels[:, out : out + POOL_GROUP] = (mixed * scale).astype(jnp.bfloat16)
+    pool_letter().start()
     for at in range(blocks):
         now = slice(at * BLOCK, (at + 1) * BLOCK)
         cum = upright[at, :, 0:heads]
@@ -464,8 +477,8 @@
         def _():
             for at in range(4):
                 tails(at).wait_send()
-            for group in range(groups):
-                chain(group).wait_send()
+            for link in range(parts):
+                chain(link).wait_send()
 
     return received, finish
 
@@ -495,16 +508,19 @@
         pltpu.make_async_copy(source, place, local_sems.at[2 + at])
         for at, (source, place) in enumerate(zip(inputs, held))
     ]
-    for at in ORDER:
+    for at in SOURCES:
         fetches[at].start()
     for load in loads:
         load.start()
+    for at in (*OTHERS, GATE):
+        fetches[at].start()
     links.barrier()
     weights = Weights(links, whole, width, (z_sends, z_arrivals), (y_sends, y_arrivals))
     work = mixers(links, tail, cores, pieces, fetches, (*held, *rest), (m_sends, m_arrivals))
 
     direct, turned = weights.direct, weights.turned
-    late = links.z >= sp_size // 2
+    both = (0, 1)
+    last = sp_size - 1
     mixed = None
     while mixed is None:
         try:
@@ -521,24 +537,37 @@
             weights.own(direct[3:4])
         elif mark == "states":
             weights.own(direct[4:])
-            weights.hop(1, direct[:1])
+            weights.turn()
+            weights.own(turned, both, (-1,))
+            pl.when(links.z >= 2)(lambda: weights.own(turned, both, (1,)))
+            weights.hop(1, direct[:1], ways=(-1,))
         elif mark == "second":
-            pl.when(late)(lambda: weights.hop(1, direct[1:3]))
+            weights.hop(1, direct[1:3], ways=(-1,))
+            pl.when(links.z == 1)(lambda: weights.own(turned, both, (1,)))
+            pl.when(links.z == 1)(lambda: weights.hop(1, direct[:4], ways=(1,)))
+            pl.when(links.z == last)(lambda: weights.hop(1, direct, ways=(1,)))
+            inner_late = jnp.logical_and(links.z >= 2, links.z < last)
+            pl.when(inner_late)(lambda: weights.hop(1, direct[:2], ways=(1,)))
         elif mark == "third":
-            pl.when(late)(lambda: weights.hop(1, direct[3:]))
+            pl.when(inner_late)(lambda: weights.hop(1, direct[2:], ways=(1,)))
+            pl.when(links.z == last)(lambda: weights.hop(2, direct[:2], ways=(1,)))
+            pl.when(links.z >= 2)(lambda: weights.hop(1, direct[3:], ways=(-1,)))
     received, finish_mixers = mixed
-    pl.when(jnp.logical_not(late))(lambda: weights.hop(1, direct[1:]))
-
-    def multiply(turn, far):
+    pl.when(links.z == 0)(lambda: weights.own(turned, both, (1,)))
+    pl.when(links.z == 1)(lambda: weights.hop(1, direct[4:], ways=(1,)))
+    pl.when(links.z <= 1)(lambda: weights.hop(1, direct[3:], ways=(-1,)))
+
+    def multiply(turn, far, sides=both):
         z = links.nearest(turn)
         source = far_channels if far else channels
 
-        @pl.loop(0, 2)
-        def _(y):
+        @pl.loop(0, len(sides))
+        def _(at):
+            y = lax.rem(links.y + sides[0] + at, 2)
             slab = z * 2 + y
-            at = pl.multiple_of(slab * width, width)
+            lanes = pl.ds(pl.multiple_of(slab * width, width), width)
             parts[far, slab] = jnp.dot(
-                source[...], whole[:, pl.ds(at, width)], preferred_element_type=jnp.float32
+                source[...], whole[:, lanes], preferred_element_type=jnp.float32
             ).astype(jnp.bfloat16)
 
             @pl.when(z // half != core)
@@ -561,13 +590,14 @@
             returned.at[slot], return_in.at[slot], o_sends, o_arrivals, slot, links.beside
         )
 
-    def give_back(turn):
+    def give_back(turn, sides=both):
         z = links.nearest(turn)
 
         @pl.when(z // half == core)
         def _():
-            @pl.loop(0, 2)
-            def _(y):
+            @pl.loop(0, len(sides))
+            def _(at):
+                y = lax.rem(links.y + sides[0] + at, 2)
                 part_letter(z, y, 1).wait_recv()
                 slot = lax.rem(z, half) * 2 + y
                 returned[slot] = (
@@ -575,32 +605,47 @@
                 ).astype(jnp.bfloat16)
                 return_letter(slot).start()
 
-    last = sp_size - 1
-    weights.turn()
+    edge = jnp.logical_or(links.z == 0, links.z == last)
     weights.settle(0)
     multiply(0, 0)
-    for step in range(2, sp_size):
-        weights.hop(step, direct)
-        if step < last:
-            weights.hop(step - 1, turned)
-            weights.settle(step - 1)
-            multiply(step - 1, 0)
+    for step in range(1, last):
+        weights.hop(step, turned, both)
+        if step + 1 < last:
+            if step == 1:
+                pl.when(links.z == last)(lambda: weights.hop(2, direct[2:]))
+                pl.when(links.z != last)(lambda: weights.hop(2, direct))
+            else:
+                weights.hop(step + 1, direct)
+            weights.settle(step)
+            multiply(step, 0)
     received()
-    for turn in range(last - 1):
+    share = -(-len(direct) // last)
+
+    def ahead(turn):
         multiply(turn, 1)
-        if turn:
-            give_back(turn - 1)
-    weights.hop(last - 1, turned)
-    weights.settle(last - 1)
-    multiply(last - 1, 1)
-    give_back(last - 2)
-    multiply(last - 1, 0)
-    give_back(last - 1)
-    weights.hop(last, turned)
+        give_back(turn)
+        multiply(turn, 0)
+
+    for turn in range(last):
+        pieces_now = direct[turn * share : (turn + 1) * share]
+        if turn == last - 1:
+            pl.when(jnp.logical_not(edge))(lambda: ahead(turn))
+            weights.settle(turn)
+            weights.hop(last, pieces_now)
+            pl.when(edge)(lambda: ahead(turn))
+        else:
+            multiply(turn, 1)
+            weights.hop(last, pieces_now)
+            give_back(turn)
+    weights.hop(last, turned, (0,))
+    multiply(last, 1, (0,))
+    multiply(last, 0, (0,))
+    give_back(last, (0,))
+    weights.hop(last, turned, (1,))
     weights.settle(last)
-    multiply(last, 1)
-    multiply(last, 0)
-    give_back(last)
+    multiply(last, 1, (1,))
+    multiply(last, 0, (1,))
+    give_back(last, (1,))
     own_half = core * half
     slots = 2 * half
 
@@ -675,7 +720,6 @@
     tok_rows, inner = x_in.shape[1:]
     wide, pool = b_in.shape[2], pool_in.shape[2]
     groups = wide // STATE
-    span = inner // groups
     blocks = tok_rows // BLOCK
     half = sp_size // cores
     slots = 2 * half
@@ -684,10 +728,10 @@
     dma = pltpu.SemaphoreType.DMA
     half_type, full_type = jnp.bfloat16, jnp.float32
     z_spots, y_spots = CHUNKS * (sp_size - 1) * 4, CHUNKS * (2 * sp_size - 1)
-    letters = 5 + groups + blocks
+    letters = 5 + CHAINS + blocks
     return pl.pallas_call(
         functools.partial(whole_kernel, sp_size, fs_size, cores, tail, pieces),
-        out_shape=jax.ShapeDtypeStruct((1, tok_rows, features // cores), half_type),
+        out_shape=pltpu.VMEM((1, tok_rows, features // cores), half_type),
         in_specs=[hbm] * (len(inputs) + 2),
         out_specs=vmem,
         scratch_shapes=[
@@ -729,16 +773,16 @@
             pltpu.VMEM((blocks, STATE, inner), full_type),
             pltpu.VMEM((STATE, inner), full_type),
             pltpu.VMEM((STATE, inner), full_type),
-            pltpu.VMEM((groups, STATE, span), half_type),
-            pltpu.VMEM((groups, STATE, span), half_type),
+            pltpu.VMEM((CHAINS, STATE, inner // CHAINS), half_type),
+            pltpu.VMEM((CHAINS, STATE, inner // CHAINS), half_type),
             pltpu.VMEM((tok_rows, inner + pool), half_type),
             pltpu.VMEM((tok_rows, inner + pool), half_type),
         ],
         compiler_params=pltpu.CompilerParams(
-            collective_id=0, has_side_effects=True, vmem_limit_bytes=54 * 2**20
+            collective_id=0, has_side_effects=True, vmem_limit_bytes=48 * 2**20
         ),
         name="paired_mixers",
-    )(*inputs, ssd_weight, pool_rows)
+    )(*(pltpu.with_memory_space_constraint(array, pltpu.HBM) for array in (*inputs, ssd_weight, pool_rows)))
 
 
 def causal_taps(input_rows, prior_rows, tap_weights, offset_bias):
@@ -816,7 +860,7 @@
                 state_output_projection,
                 jnp.swapaxes(step_size_input, 1, 2),
                 jnp.swapaxes(added_log_decay, 1, 2),
-                logarithm_rates[:, None],
+                logarithm_rates[None],
                 head_channel_taps,
                 input_projection_taps,
                 output_projection_taps,

time: 94 us -> 85.3 us (0.907)
  the two profiles are of different devices: /device:TPU:0 before, /device:TPU:25 now
where the time goes in v3:
time: 85.3 us; the launch traced here: 85.1 us
  Pallas kernels  82.5 us (97%)
  local copies, waits for them, and re-layouts  1.77 us (2%)
    pallas_call x1, Pallas kernels, mixed_and_projected(): pl.pallas_call(functools.partial(whole_kernel, sp_size, fs_size, cores, t...  82.5 us

profile of v3, /device:TPU:25, one launch (start us, length us, event | category | flops | bytes accessed | tf_op | source)
XLA Modules:
  0.0 85.1 jit_solution(5363575432933299791)
XLA Ops:
  0.0 0.8 pad_maximum_fusion
  0.8 0.6 broadcast_in_dim.7.refs_10_
  1.4 82.5 %paired_mixers.1 = bf16[1,384,2048]{2,1,0:T(8,128)(2,1)S(1)} custom-call(bf16[1,384,1024]{2,1,0:T(8,128)(2,1)} %refs_0_.1, bf16[1,384,1024]{2,1,0:T(8,128)(2,1)} %refs_1_.1, bf16[1,384,256]{2,1,0:T(8,128)(2,1)} %refs_2_.1, bf16[1,384,256]{2,1,0:T(8,128)(2,1)} %refs_3_.1, bf16[1,16,384]{2,1,0:T(8,128)(2,1)} %bitcast.4, f32[1,16,384]{2,1,0:T(8,128)} %bitcast.3, ...), custom_call_target="tpu_custom_call" | custom-call | tf_op jit(solution)/shard_map/paired_mixers/pallas_call | solution.py:732
  83.9 1.1 %copy.20 = bf16[1,384,2048]{2,1,0:T(8,128)(2,1)} copy(bf16[1,384,2048]{2,1,0:T(8,128)(2,1)S(1)} %paired_mixers.1) | data formatting | bytes 3145728

commit v4 on v3

--- a/solution.py
+++ b/solution.py
@@ -48,8 +48,9 @@
 MESH_IDS = pl.DeviceIdType.MESH
 EXACT = lax.Precision.HIGHEST
 CHUNKS, CHAINS = 6, 4
-INPUTS, GATE, VECTORS = 13, 1, 10
-SOURCES, OTHERS = (0, 2, 3, 11), (4, 5, 6, 7, 8, 9, 10, 12)
+NAMES = ("out", "gain", "scale", "bias")
+INPUTS, GATE, VECTORS = 16, 1, 12
+SOURCES, OTHERS = (0, 2, 3, 10), (4, 5, 6, 7, 8, 9, 11, 12, 13, 14, 15)
 
 
 class Links:
@@ -190,6 +191,11 @@
     return jnp.maximum(rows, 0.0) + jnp.log(1.0 + jnp.exp(-jnp.abs(rows)))
 
 
+def piece(vector, offset, size):
+    at = pl.multiple_of(offset, 128)
+    return vector[pl.ds(at, size)].astype(jnp.float32)[None]
+
+
 def chosen(core, options):
     best = options[0]
     for at in range(1, len(options)):
@@ -197,8 +203,8 @@
     return best
 
 
-def mixers(links, tail, cores, pieces, fetches, refs, sems):
-    (x_in, gate, b_in, c_in, dt, added, rates, x_taps, b_taps, c_taps, vectors, pool_in,
+def mixers(links, tail, cores, vectors, fetches, refs, sems):
+    (x_in, gate, b_in, c_in, dt, added, rates, x_taps, b_taps, c_taps, pool_in,
      pool_weight, prior_x, prior_b, prior_c, prior_pool, x_pad, bc_pad, pool_pad,
      pool_two, pool_four, x_split, bc_conv, b_turned, flat, upright, within, grown, local_in,
      state, before, carry_in, carry_out, channels, far_channels) = refs
@@ -240,6 +246,7 @@
         )
 
     follows = z + 1 < links.n
+    yield "loaded"
     for at in SOURCES:
         fetches[at].wait()
 
@@ -278,7 +285,7 @@
 
     taps_x = mine(x_taps, inner)
     taps_bc = jnp.concatenate([mine(b_taps, wide), mine(c_taps, wide)], axis=1)
-    bias_b = pieces(vectors, "bias", core * wide, wide)
+    bias_b = piece(vectors["bias"], core * wide, wide)
     bias_bc = jnp.concatenate([bias_b, jnp.zeros_like(bias_b)], axis=1)
 
     @pl.when(z == 0)
@@ -408,7 +415,7 @@
             pool_weight[core * pool_groups + group],
             preferred_element_type=jnp.float32,
         )
-        scale = pieces(vectors, "scale", core * pool + group * POOL_GROUP, POOL_GROUP)
+        scale = piece(vectors["scale"], core * pool + group * POOL_GROUP, POOL_GROUP)
         out = inner + group * POOL_GROUP
         channels[:, out : out + POOL_GROUP] = (mixed * scale).astype(jnp.bfloat16)
     pool_letter().start()
@@ -458,7 +465,7 @@
                 gate[0, now, cols].astype(jnp.float32)
             )
             root = lax.rsqrt(jnp.mean(mixed * mixed, axis=1, keepdims=True) + eps)
-            gain = pieces(vectors, "gain", core * inner + group * span, span)
+            gain = piece(vectors["gain"], core * inner + group * span, span)
             channels[now, cols] = (mixed * root * gain).astype(jnp.bfloat16)
             end = ends[at][group]
             falling[group] = end if at == 0 else falling[group] * end
@@ -483,13 +490,14 @@
     return received, finish
 
 
-def whole_kernel(sp_size, fs_size, cores, tail, pieces, *refs):
+def whole_kernel(sp_size, fs_size, cores, tail, *refs):
     inputs, ssd_weight, pool_rows, out = refs[:INPUTS], *refs[INPUTS : INPUTS + 3]
     (z_sends, z_arrivals, y_sends, y_arrivals, m_sends, m_arrivals, p_sends, p_arrivals, o_sends,
      o_arrivals, local_sems, whole, parts, part_in, returned, return_in, squares, squares_in,
      *rest) = refs[INPUTS + 3 :]
     held, rest = rest[:INPUTS], rest[INPUTS:]
-    vectors = held[VECTORS]
+    vectors = dict(zip(NAMES, held[VECTORS:]))
+    held = held[:VECTORS]
     channels, far_channels = rest[-2:]
     links = Links(sp_size, fs_size)
     width = ssd_weight.shape[1]
@@ -506,17 +514,15 @@
     ]
     fetches = [
         pltpu.make_async_copy(source, place, local_sems.at[2 + at])
-        for at, (source, place) in enumerate(zip(inputs, held))
+        for at, (source, place) in enumerate(zip(inputs, (*held, *vectors.values())))
     ]
-    for at in SOURCES:
-        fetches[at].start()
     for load in loads:
         load.start()
-    for at in (*OTHERS, GATE):
+    for at in (*SOURCES, *OTHERS, GATE):
         fetches[at].start()
     links.barrier()
     weights = Weights(links, whole, width, (z_sends, z_arrivals), (y_sends, y_arrivals))
-    work = mixers(links, tail, cores, pieces, fetches, (*held, *rest), (m_sends, m_arrivals))
+    work = mixers(links, tail, cores, vectors, fetches, (*held, *rest), (m_sends, m_arrivals))
 
     direct, turned = weights.direct, weights.turned
     both = (0, 1)
@@ -528,18 +534,20 @@
         except StopIteration as ended:
             mixed = ended.value
             break
-        if mark == "start":
+        if mark == "loaded":
             for load in loads:
                 load.wait()
             weights.begin()
-            weights.own(direct[:3])
+            weights.own(direct[:3], ways=(-1,))
+        elif mark == "start":
+            weights.own(direct[:3], ways=(1,))
         elif mark == 1:
             weights.own(direct[3:4])
         elif mark == "states":
             weights.own(direct[4:])
             weights.turn()
             weights.own(turned, both, (-1,))
-            pl.when(links.z >= 2)(lambda: weights.own(turned, both, (1,)))
+            pl.when(links.z == last)(lambda: weights.own(turned, both, (1,)))
             weights.hop(1, direct[:1], ways=(-1,))
         elif mark == "second":
             weights.hop(1, direct[1:3], ways=(-1,))
@@ -547,9 +555,10 @@
             pl.when(links.z == 1)(lambda: weights.hop(1, direct[:4], ways=(1,)))
             pl.when(links.z == last)(lambda: weights.hop(1, direct, ways=(1,)))
             inner_late = jnp.logical_and(links.z >= 2, links.z < last)
-            pl.when(inner_late)(lambda: weights.hop(1, direct[:2], ways=(1,)))
+            pl.when(inner_late)(lambda: weights.hop(1, direct[:3], ways=(1,)))
         elif mark == "third":
-            pl.when(inner_late)(lambda: weights.hop(1, direct[2:], ways=(1,)))
+            pl.when(inner_late)(lambda: weights.own(turned, both, (1,)))
+            pl.when(inner_late)(lambda: weights.hop(1, direct[3:], ways=(1,)))
             pl.when(links.z == last)(lambda: weights.hop(2, direct[:2], ways=(1,)))
             pl.when(links.z >= 2)(lambda: weights.hop(1, direct[3:], ways=(-1,)))
     received, finish_mixers = mixed
@@ -688,7 +697,7 @@
             (return_in[slot].astype(jnp.float32), 1 - links.x),
         ):
             at = pl.multiple_of((first + x) * width, width)
-            gain = pieces(vectors, "out", core * out.shape[2] + at, width)
+            gain = piece(vectors["out"], core * out.shape[2] + at, width)
             out[0, :, pl.ds(at, width)] = (values * root * gain).astype(jnp.bfloat16)
 
     exchange.wait_send()
@@ -707,16 +716,8 @@
     sp_size, fs_size, cores = lax.axis_size("sp"), lax.axis_size("fs"), lax.axis_size("tp")
     width = ssd_weight.shape[1]
     x_in, b_in, pool_in = inputs[0], inputs[2], inputs[10]
-    starts, features = {}, vectors["out"].shape[0]
-    for name, vector in vectors.items():
-        starts[name] = sum(vectors[other].shape[0] for other in starts)
-
-    def pieces(ref, name, offset, size):
-        at = pl.multiple_of(starts[name] + offset, 128)
-        return ref[:, pl.ds(at, size)].astype(jnp.float32)
-
-    joined = jnp.concatenate(list(vectors.values()))[None]
-    inputs = (*inputs[:10], joined, *inputs[10:])
+    features = vectors["out"].shape[0]
+    inputs = (*inputs, *(vectors[name] for name in NAMES))
     tok_rows, inner = x_in.shape[1:]
     wide, pool = b_in.shape[2], pool_in.shape[2]
     groups = wide // STATE
@@ -730,7 +731,7 @@
     z_spots, y_spots = CHUNKS * (sp_size - 1) * 4, CHUNKS * (2 * sp_size - 1)
     letters = 5 + CHAINS + blocks
     return pl.pallas_call(
-        functools.partial(whole_kernel, sp_size, fs_size, cores, tail, pieces),
+        functools.partial(whole_kernel, sp_size, fs_size, cores, tail),
         out_shape=pltpu.VMEM((1, tok_rows, features // cores), half_type),
         in_specs=[hbm] * (len(inputs) + 2),
         out_specs=vmem,

time: 85.3 us -> 82.3 us (0.965)
  Pallas kernels: 82.5 us -> 81 us
    pallas_call x1, Pallas kernels: 82.5 us -> 81 us  [mixed_and_projected(): pl.pallas_call(functools.partial(whole_kernel, sp_size, fs_size, cores, t...]
where the time goes in v4:
time: 82.3 us; the launch traced here: 82.1 us
  Pallas kernels  81 us (98%)
  local copies, waits for them, and re-layouts  1.15 us (1%)
    pallas_call x1, Pallas kernels, mixed_and_projected(): pl.pallas_call(functools.partial(whole_kernel, sp_size, fs_size, cores, t...  81 us

profile of v4, /device:TPU:25, one launch (start us, length us, event | category | flops | bytes accessed | tf_op | source)
XLA Modules:
  0.0 82.1 jit_solution(539245258051489902)
XLA Ops:
  0.0 81.0 %paired_mixers.1 = bf16[1,384,2048]{2,1,0:T(8,128)(2,1)S(1)} custom-call(bf16[1,384,1024]{2,1,0:T(8,128)(2,1)} %refs_0_.1, bf16[1,384,1024]{2,1,0:T(8,128)(2,1)} %refs_1_.1, bf16[1,384,256]{2,1,0:T(8,128)(2,1)} %refs_2_.1, bf16[1,384,256]{2,1,0:T(8,128)(2,1)} %refs_3_.1, bf16[1,16,384]{2,1,0:T(8,128)(2,1)} %bitcast.4, f32[1,16,384]{2,1,0:T(8,128)} %bitcast.3, ...), custom_call_target="tpu_custom_call" | custom-call | tf_op jit(solution)/shard_map/paired_mixers/pallas_call | solution.py:733
  81.0 1.1 %copy.20 = bf16[1,384,2048]{2,1,0:T(8,128)(2,1)} copy(bf16[1,384,2048]{2,1,0:T(8,128)(2,1)S(1)} %paired_mixers.1) | data formatting | bytes 3145728

commit v5 on v4

--- a/solution.py
+++ b/solution.py
@@ -559,7 +559,7 @@
         elif mark == "third":
             pl.when(inner_late)(lambda: weights.own(turned, both, (1,)))
             pl.when(inner_late)(lambda: weights.hop(1, direct[3:], ways=(1,)))
-            pl.when(links.z == last)(lambda: weights.hop(2, direct[:2], ways=(1,)))
+            pl.when(links.z == last)(lambda: weights.hop(2, direct[:3], ways=(1,)))
             pl.when(links.z >= 2)(lambda: weights.hop(1, direct[3:], ways=(-1,)))
     received, finish_mixers = mixed
     pl.when(links.z == 0)(lambda: weights.own(turned, both, (1,)))
@@ -621,7 +621,7 @@
         weights.hop(step, turned, both)
         if step + 1 < last:
             if step == 1:
-                pl.when(links.z == last)(lambda: weights.hop(2, direct[2:]))
+                pl.when(links.z == last)(lambda: weights.hop(2, direct[3:]))
                 pl.when(links.z != last)(lambda: weights.hop(2, direct))
             else:
                 weights.hop(step + 1, direct)
@@ -653,8 +653,8 @@
     weights.hop(last, turned, (1,))
     weights.settle(last)
     multiply(last, 1, (1,))
+    give_back(last, (1,))
     multiply(last, 0, (1,))
-    give_back(last, (1,))
     own_half = core * half
     slots = 2 * half
 

time: 82.3 us -> 81.5 us (level)
  no operation moved by 1% of the time
where the time goes in v5:
time: 81.5 us; the launch traced here: 81.4 us
  Pallas kernels  80.2 us (98%)
  local copies, waits for them, and re-layouts  1.15 us (1%)
    pallas_call x1, Pallas kernels, mixed_and_projected(): pl.pallas_call(functools.partial(whole_kernel, sp_size, fs_size, cores, t...  80.2 us

profile of v5, /device:TPU:25, one launch (start us, length us, event | category | flops | bytes accessed | tf_op | source)
XLA Modules:
  0.0 81.4 jit_solution(7232429317186061259)
XLA Ops:
  0.0 80.2 %paired_mixers.1 = bf16[1,384,2048]{2,1,0:T(8,128)(2,1)S(1)} custom-call(bf16[1,384,1024]{2,1,0:T(8,128)(2,1)} %refs_0_.1, bf16[1,384,1024]{2,1,0:T(8,128)(2,1)} %refs_1_.1, bf16[1,384,256]{2,1,0:T(8,128)(2,1)} %refs_2_.1, bf16[1,384,256]{2,1,0:T(8,128)(2,1)} %refs_3_.1, bf16[1,16,384]{2,1,0:T(8,128)(2,1)} %bitcast.4, f32[1,16,384]{2,1,0:T(8,128)} %bitcast.3, ...), custom_call_target="tpu_custom_call" | custom-call | tf_op jit(solution)/shard_map/paired_mixers/pallas_call | solution.py:733
  80.2 1.1 %copy.20 = bf16[1,384,2048]{2,1,0:T(8,128)(2,1)} copy(bf16[1,384,2048]{2,1,0:T(8,128)(2,1)S(1)} %paired_mixers.1) | data formatting | bytes 3145728

commit v6 on v5

--- a/solution.py
+++ b/solution.py
@@ -689,7 +689,7 @@
     features = cores * out.shape[2]
     root = lax.rsqrt(row_squares / features + eps)
 
-    @pl.loop(0, slots)
+    @pl.loop(0, slots, unroll=True)
     def _(slot):
         first = (slot // 2) * fs_size + 2 * lax.rem(slot, 2)
         for values, x in (

time: 81.5 us -> 81.4 us (level)
  no operation moved by 1% of the time
where the time goes in v6:
time: 81.4 us; the launch traced here: 81.3 us
  Pallas kernels  80.1 us (98%)
  local copies, waits for them, and re-layouts  1.15 us (1%)
    pallas_call x1, Pallas kernels, mixed_and_projected(): pl.pallas_call(functools.partial(whole_kernel, sp_size, fs_size, cores, t...  80.1 us

profile of v6, /device:TPU:25, one launch (start us, length us, event | category | flops | bytes accessed | tf_op | source)
XLA Modules:
  0.0 81.3 jit_solution(2535421852464785795)
XLA Ops:
  0.0 80.1 %paired_mixers.1 = bf16[1,384,2048]{2,1,0:T(8,128)(2,1)S(1)} custom-call(bf16[1,384,1024]{2,1,0:T(8,128)(2,1)} %refs_0_.1, bf16[1,384,1024]{2,1,0:T(8,128)(2,1)} %refs_1_.1, bf16[1,384,256]{2,1,0:T(8,128)(2,1)} %refs_2_.1, bf16[1,384,256]{2,1,0:T(8,128)(2,1)} %refs_3_.1, bf16[1,16,384]{2,1,0:T(8,128)(2,1)} %bitcast.4, f32[1,16,384]{2,1,0:T(8,128)} %bitcast.3, ...), custom_call_target="tpu_custom_call" | custom-call | tf_op jit(solution)/shard_map/paired_mixers/pallas_call | solution.py:733
  80.1 1.1 %copy.20 = bf16[1,384,2048]{2,1,0:T(8,128)(2,1)} copy(bf16[1,384,2048]{2,1,0:T(8,128)(2,1)S(1)} %paired_mixers.1) | data formatting | bytes 3145728
